TPU v7x, 768 devices: a whole 4x8x12 slice. The times are simulated.
768 devices in a mesh: sp: 12 (over z), tp: 8 (over y), dp: 8 (over x, core).
Axes of the slice: x: 4, y: 8, z: 12, core: 2. Of those that a mesh axis runs over, the one named last changes fastest.
Arguments:
- latent: bfloat16 [30720, 3072], P(('dp', 'sp', 'tp')), parts along dimension 0, may hold values from -6 to 6
- condition: float32 [24576], P('dp'), parts along dimension 0, may hold values from -8 to 8
- ctx_condition: float32 [3072], replicated, may hold values from -8 to 8
- context: bfloat16 [3072, 3072], P(('dp', 'sp')), parts along dimension 0, may hold values from -6 to 6
- mod_shift: bfloat16 [3072, 3072], P('sp', 'tp'), may hold values from -0.109375 to 0.109375
- mod_scale: bfloat16 [3072, 3072], P('sp', 'tp'), may hold values from -0.109375 to 0.109375
- mod_gate: bfloat16 [3072, 3072], P('sp', 'tp'), may hold values from -0.109375 to 0.109375
- norm_gain: float32 [3072], replicated, may hold values from 0.5 to 6
- w_query: bfloat16 [3072, 3072], P(None, 'tp'), may hold values from -0.109375 to 0.109375
- key_weight: bfloat16 [3072, 512], P(None, 'tp'), may hold values from -0.109375 to 0.109375
- value_weight: bfloat16 [3072, 512], P(None, 'tp'), may hold values from -0.109375 to 0.109375
- w_gate: bfloat16 [3072, 3072], P(None, 'tp'), may hold values from -0.109375 to 0.109375
- w_out: bfloat16 [3072, 3072], P('tp'), may hold values from -1.5 to 1.5
- sink_logit: float32 [48], P('tp'), may hold values from 4 to 7.5
Outputs:
- updated_latent: bfloat16 [30720, 3072], P(('dp', 'sp', 'tp')), parts along dimension 0
There are 8 independent parts, one for each index of `dp`. A program takes and returns all parts, laid end to end along the dimension named above; an argument that names none is the same for every part. Nothing has to cross between parts.
All inputs are finite; a program needn't handle non-finite values.
Results may differ from a plain program's by a relative error of at most 0.02.
The roundings to bfloat16 on the way count: a program that leaves them out, or rounds other values in their place, can miss the bound.
Values may be sent and summed in bfloat16 or wider, within the bound.
No kernel may reach another device: no remote copies, remote signals or barrier semaphores. Data moves between devices by JAX's collectives and lax.ppermute only.
A program may use at most 64 MiB of HBM per device.

v0:
```python
import math

import jax
import jax.numpy as jnp
from jax import lax
from jax.sharding import PartitionSpec as P

HEAD_SIZE = 64
WINDOW = 128
GRID_W = 64


NORM_EPS = 1e-06
MASK_VALUE = -1e30


def copy_for_each(shard, axis):
    copies = jnp.broadcast_to(shard, (lax.axis_size(axis), *shard.shape))
    return lax.all_to_all(copies, axis, split_axis=0, concat_axis=0, tiled=True)


def taken_together(shard, axis):
    everything = copy_for_each(shard, axis)
    return jnp.sum(everything, axis=0)


def laid_out(tiles, dim):
    tiles = jnp.moveaxis(tiles, 0, dim)
    lengths = tiles.shape
    return tiles.reshape(*lengths[:dim], lengths[dim] * lengths[dim + 1], *lengths[dim + 2 :])


def gather_directly(shard, axis, dim):
    return laid_out(copy_for_each(shard, axis), dim)


def with_halo(block, sides, width):
    for axis, dim in sides:
        count = lax.axis_size(axis)
        forward = [(i, i + 1) for i in range(count - 1)]
        backward = [(target, source) for source, target in forward]
        low = lax.ppermute(
            lax.slice_in_dim(block, block.shape[dim] - width, None, axis=dim), axis, forward
        )
        high = lax.ppermute(lax.slice_in_dim(block, 0, width, axis=dim), axis, backward)
        block = jnp.concatenate([low, block, high], axis=dim)
    return block


def cut_along(shard, dim, size):
    before, after = (shard.shape[:dim], shard.shape[dim + 1 :])
    return jnp.moveaxis(shard.reshape(*before, size, -1, *after), dim, 0)


def sum_at_owner(shard, axis, dim):
    size = lax.axis_size(axis)
    tiles = lax.all_to_all(cut_along(shard, dim, size), axis, 0, 0, tiled=True)
    return jnp.sum(tiles.astype(jnp.float32), axis=0)


def modulate(row_data, gain_vec, shift_vec, scale_vec):
    values = row_data.astype(jnp.float32)
    inverse = lax.rsqrt(jnp.mean(values * values, axis=-1, keepdims=True) + NORM_EPS)
    return (values * inverse * gain_vec * (1.0 + scale_vec) + shift_vec).astype(jnp.bfloat16)


def rotate(projected, positions):
    row_count = projected.shape[0]
    head_count = projected.shape[1] // HEAD_SIZE
    quarter = HEAD_SIZE // 4
    half_dim = HEAD_SIZE // 2
    inverse = jnp.exp(-math.log(10000.0) * jnp.arange(quarter, dtype=jnp.float32) / quarter)
    grid_row = (positions // GRID_W).astype(jnp.float32)
    mesh_column = (positions % GRID_W).astype(jnp.float32)
    angles = jnp.concatenate([grid_row[:, None] * inverse, mesh_column[:, None] * inverse], axis=1)
    cosine = jnp.cos(angles)[:, None, :]
    sine_table = jnp.sin(angles)[:, None, :]
    shaped = projected.reshape(row_count, head_count, HEAD_SIZE)
    first_half = shaped[..., :half_dim]
    second = shaped[..., half_dim:]
    turned = jnp.concatenate(
        [first_half * cosine - second * sine_table, second * cosine + first_half * sine_table],
        axis=-1,
    )
    return turned.reshape(row_count, head_count * HEAD_SIZE)


def attend(
    queries, key_rows, value_rows, ctx_keys, ctx_values, sink_logit, q_begin, k_begin, seq_total
):
    row_count = queries.shape[0]
    key_count = key_rows.shape[0]
    ctx_count = ctx_keys.shape[0]
    kv_heads = key_rows.shape[1] // HEAD_SIZE
    head_count = queries.shape[1] // HEAD_SIZE
    group_size = head_count // kv_heads
    factor = 1.0 / math.sqrt(HEAD_SIZE)
    q_heads = queries.reshape(row_count, kv_heads, group_size, HEAD_SIZE)
    k_heads = key_rows.reshape(key_count, kv_heads, HEAD_SIZE)
    v_heads = value_rows.reshape(key_count, kv_heads, HEAD_SIZE)
    ck_heads = ctx_keys.reshape(ctx_count, kv_heads, HEAD_SIZE)
    cv_heads = ctx_values.reshape(ctx_count, kv_heads, HEAD_SIZE)
    near_scores = (
        jnp.einsum("qkgd,skd->kgqs", q_heads, k_heads, preferred_element_type=jnp.float32) * factor
    )
    q_pos = q_begin + jnp.arange(row_count, dtype=jnp.int32)
    k_pos = k_begin + jnp.arange(key_count, dtype=jnp.int32)
    in_window = (jnp.abs(q_pos[:, None] - k_pos[None, :]) <= WINDOW) & (
        (k_pos >= 0) & (k_pos < seq_total)
    )[None, :]
    near_scores = jnp.where(in_window, near_scores, MASK_VALUE)
    ctx_scores = (
        jnp.einsum("qkgd,skd->kgqs", q_heads, ck_heads, preferred_element_type=jnp.float32) * factor
    )
    sink_score = sink_logit.reshape(kv_heads, group_size)[:, :, None, None]
    peak_score = jnp.maximum(
        jnp.maximum(
            jnp.max(near_scores, axis=-1, keepdims=True),
            jnp.max(ctx_scores, axis=-1, keepdims=True),
        ),
        sink_score,
    )
    near_exp = jnp.exp(near_scores - peak_score)
    ctx_exp = jnp.exp(ctx_scores - peak_score)
    softmax_denominator = (
        jnp.sum(near_exp, axis=-1, keepdims=True)
        + jnp.sum(ctx_exp, axis=-1, keepdims=True)
        + jnp.exp(sink_score - peak_score)
    )
    near_weights = (near_exp / softmax_denominator).astype(jnp.bfloat16)
    ctx_weights = (ctx_exp / softmax_denominator).astype(jnp.bfloat16)
    result = jnp.einsum("kgqs,skd->qkgd", near_weights, v_heads, preferred_element_type=jnp.float32)
    result = result + jnp.einsum(
        "kgqs,skd->qkgd", ctx_weights, cv_heads, preferred_element_type=jnp.float32
    )
    return result.reshape(row_count, head_count * HEAD_SIZE)


def shards(
    latent,
    condition,
    ctx_condition,
    context,
    mod_shift,
    mod_scale,
    mod_gate,
    norm_gain,
    w_query,
    key_weight,
    value_weight,
    w_gate,
    w_out,
    sink_logit,
):
    sp_count = lax.axis_size("sp")
    sp_rank = lax.axis_index("sp")
    mod_rows = mod_shift.shape[0]
    cond_act = jax.nn.silu(condition).astype(jnp.bfloat16)
    ctx_act = jax.nn.silu(ctx_condition).astype(jnp.bfloat16)
    first_row = sp_rank * mod_rows
    lat_piece = lax.dynamic_slice_in_dim(cond_act, first_row, mod_rows, 0)
    ctx_piece = lax.dynamic_slice_in_dim(ctx_act, first_row, mod_rows, 0)
    both_conds = jnp.stack([lat_piece, ctx_piece])
    partial_value = jnp.concatenate(
        [
            jnp.dot(both_conds, mod_shift, preferred_element_type=jnp.float32),
            jnp.dot(both_conds, mod_scale, preferred_element_type=jnp.float32),
            jnp.dot(lat_piece[None, :], mod_gate, preferred_element_type=jnp.float32),
        ],
        axis=0,
    )
    summed = taken_together(partial_value, "sp")
    vectors = gather_directly(summed, "tp", 1)
    lat_shift = vectors[0]
    ctx_shift = vectors[1]
    lat_scale = vectors[2]
    ctx_scale = vectors[3]
    lat_gate = vectors[4]
    hidden = modulate(latent, norm_gain, lat_shift, lat_scale)
    ctx_hidden = modulate(context, norm_gain, ctx_shift, ctx_scale)
    kv_width = key_weight.shape[1]
    q_width = w_query.shape[1]
    ctx_pair = jnp.concatenate(
        [
            jnp.dot(ctx_hidden, key_weight, preferred_element_type=jnp.float32).astype(
                jnp.bfloat16
            ),
            jnp.dot(ctx_hidden, value_weight, preferred_element_type=jnp.float32).astype(
                jnp.bfloat16
            ),
        ],
        axis=1,
    )
    ctx_all = gather_directly(ctx_pair, "sp", 0)
    row_piece = lax.all_gather(hidden, "tp", axis=0, tiled=True)
    projected = jnp.concatenate(
        [
            jnp.dot(row_piece, w_query, preferred_element_type=jnp.float32),
            jnp.dot(row_piece, key_weight, preferred_element_type=jnp.float32),
            jnp.dot(row_piece, value_weight, preferred_element_type=jnp.float32),
            jnp.dot(row_piece, w_gate, preferred_element_type=jnp.float32),
        ],
        axis=1,
    )
    block_rows = projected.shape[0]
    q_begin = sp_rank * block_rows
    positions = q_begin + jnp.arange(block_rows, dtype=jnp.int32)
    queries = rotate(projected[:, :q_width], positions).astype(jnp.bfloat16)
    key_rows = rotate(projected[:, q_width : q_width + kv_width], positions).astype(jnp.bfloat16)
    value_rows = projected[:, q_width + kv_width : q_width + 2 * kv_width].astype(jnp.bfloat16)
    gate_proj = projected[:, q_width + 2 * kv_width :].astype(jnp.bfloat16)
    key_value = jnp.concatenate([key_rows, value_rows], axis=1)
    padded = with_halo(key_value, (("sp", 0),), WINDOW)
    attended = attend(
        queries,
        padded[:, :kv_width],
        padded[:, kv_width:],
        ctx_all[:, :kv_width],
        ctx_all[:, kv_width:],
        sink_logit,
        q_begin,
        q_begin - WINDOW,
        block_rows * sp_count,
    )
    mixed = (attended * jax.nn.silu(gate_proj.astype(jnp.float32))).astype(jnp.bfloat16)
    branch = sum_at_owner(
        jnp.dot(mixed, w_out, preferred_element_type=jnp.float32).astype(jnp.bfloat16), "tp", 0
    )
    return (latent.astype(jnp.float32) + lat_gate * branch).astype(jnp.bfloat16)


def solution(mesh):
    return jax.shard_map(
        shards,
        mesh=mesh,
        in_specs=(
            P(("dp", "sp", "tp"), None),
            P("dp"),
            P(),
            P(("dp", "sp"), None),
            P("sp", "tp"),
            P("sp", "tp"),
            P("sp", "tp"),
            P(),
            P(None, "tp"),
            P(None, "tp"),
            P(None, "tp"),
            P(None, "tp"),
            P("tp", None),
            P("tp"),
        ),
        out_specs=P(("dp", "sp", "tp"), None),
        check_vma=False,
    )
```

profile of v0, /device:TPU:196, one launch (start us, length us, event | category | flops | bytes accessed | tf_op | source)
XLA Modules:
  0.0 175.8 jit_solution(12286617849738092318)
XLA Ops:
  7.5 1.2 fusion.47
  8.7 1.1 fusion.48
  9.7 1.1 fusion.52
  11.5 13.0 %all-to-all-start = ((f32[12,5,384]{2,1,0:T(8,128)}), f32[12,5,384]{2,1,0:T(8,128)S(1)}, u32[]{:S(2)}, u32[]{:S(2)}) async-start(f32[12,5,384]{2,1,0:T(8,128)} %broadcast_in_dim.12), calls=%async_computation | async-start | bytes 294912 | tf_op jit(solution)/shard_map/all_to_all | solution.py:19
  24.5 1.1 fusion.14
  25.6 8.7 %all-to-all-done = f32[12,5,384]{2,1,0:T(8,128)S(1)} async-done(((f32[12,5,384]{2,1,0:T(8,128)}), f32[12,5,384]{2,1,0:T(8,128)S(1)}, u32[]{:S(2)}, u32[]{:S(2)}) %all-to-all-start) | async-done | bytes 92192 | tf_op jit(solution)/shard_map/all_to_all | solution.py:19
  35.0 7.1 %all-to-all-start.1 = ((f32[8,5,384]{2,1,0:T(8,128)}), f32[8,5,384]{2,1,0:T(8,128)S(1)}, u32[]{:S(2)}, u32[]{:S(2)}) async-start(f32[8,5,384]{2,1,0:T(8,128)} %broadcast_in_dim.13), calls=%async_computation.1 | async-start | bytes 196608 | tf_op jit(solution)/shard_map/all_to_all | solution.py:19
  42.1 8.7 %all-to-all-done.1 = f32[8,5,384]{2,1,0:T(8,128)S(1)} async-done(((f32[8,5,384]{2,1,0:T(8,128)}), f32[8,5,384]{2,1,0:T(8,128)S(1)}, u32[]{:S(2)}, u32[]{:S(2)}) %all-to-all-start.1) | async-done | bytes 61472 | tf_op jit(solution)/shard_map/all_to_all | solution.py:19
  51.5 1.8 %fusion.18 = bf16[40,3072]{1,0:T(8,128)(2,1)} fusion(bf16[40,3072]{1,0:T(8,128)(2,1)} %param.14, f32[3072]{0:T(1024)S(1)} %bitcast.99, f32[3072]{0:T(1024)S(1)} %bitcast.100, f32[3072]{0:T(1024)} %param.21, f32[40]{0:T(128)S(1)} %add_rsqrt_fusion.1), kind=kLoop, calls=%fused_computation.33 | loop fusion | flops 737280 | bytes 528544 | tf_op jit(solution)/shard_map/convert_element_type | solution.py:64
  55.4 1.0 convolution_convert_fusion.3
  56.4 1.0 convolution_convert_fusion.4
  58.2 6.4 %all-to-all-start.2 = ((bf16[12,32,128]{2,1,0:T(8,128)(2,1)}), bf16[12,32,128]{2,1,0:T(8,128)(2,1)S(1)}, u32[]{:S(2)}, u32[]{:S(2)}) async-start(bf16[12,32,128]{2,1,0:T(8,128)(2,1)} %broadcast_in_dim.16), calls=%async_computation.2 | async-start | bytes 196608 | tf_op jit(solution)/shard_map/all_to_all | solution.py:19
  64.6 26.9 %all-gather.2.cloned.1.call-done = bf16[320,3072]{1,0:T(8,128)(2,1)} async-done(((bf16[40,3072]{1,0:T(8,128)(2,1)}), bf16[320,3072]{1,0:T(8,128)(2,1)}) %all-gather.2.cloned.1.call-update) | async-done | bytes 1966096 | tf_op jit(solution)/shard_map/all_gather | solution.py:195
  91.5 2.4 %convolution_bitcast_fusion = f32[320,1,64]{0,2,1:T(8,128)S(1)} fusion(bf16[320,3072]{1,0:T(8,128)(2,1)} %all-gather.2.cloned.1.call-done, bf16[3072,64]{0,1:T(8,128)(2,1)S(1)} %copy-done.3), kind=kOutput, calls=%fused_computation.20 | convolution fusion | flops 125829120 | bytes 2441216 | tf_op jit(solution)/shard_map/dot_general | solution.py:199
  95.8 4.8 %collective-permute-start = (bf16[128,128]{0,1:T(8,128)(2,1)S(1)}, bf16[128,128]{0,1:T(8,128)(2,1)S(1)}, u32[]{:S(2)}, u32[]{:S(2)}) collective-permute-start(bf16[128,128]{0,1:T(8,128)(2,1)S(1)} %get-tuple-element.14), channel_id=1, source_target_pairs={{0,64},{64,128},{128,192},{192,256},{256,320},{320,384},{384,448},... | collective-permute-start | bytes 98312 | tf_op jit(solution)/shard_map/ppermute | solution.py:42
  100.6 2.2 %collective-permute-start.1 = (bf16[128,128]{0,1:T(8,128)(2,1)S(1)}, bf16[128,128]{0,1:T(8,128)(2,1)S(1)}, u32[]{:S(2)}, u32[]{:S(2)}) collective-permute-start(bf16[128,128]{0,1:T(8,128)(2,1)S(1)} %get-tuple-element.15), channel_id=1, source_target_pairs={{64,0},{128,64},{192,128},{256,192},{320,256},{384,320},{448,384},... | collective-permute-start | bytes 98312 | tf_op jit(solution)/shard_map/ppermute | solution.py:45
  102.8 1.5 fusion.53
  105.2 2.5 %collective-permute-done.1 = bf16[128,128]{0,1:T(8,128)(2,1)S(1)} collective-permute-done((bf16[128,128]{0,1:T(8,128)(2,1)S(1)}, bf16[128,128]{0,1:T(8,128)(2,1)S(1)}, u32[]{:S(2)}, u32[]{:S(2)}) %collective-permute-start.1) | collective-permute-done | bytes 32800 | tf_op jit(solution)/shard_map/ppermute | solution.py:45
  107.8 1.2 fusion.1
  110.0 1.3 fusion
  111.4 1.1 fusion.6
  112.6 1.6 fusion.9
  115.1 5.9 %convolution_convert_fusion = bf16[320,3072]{1,0:T(8,128)(2,1)} fusion(bf16[384,3072]{1,0:T(8,128)(2,1)S(1)} %copy-done, f32[320,384]{1,0:T(8,128)} %copy.31, bf16[320,3072]{1,0:T(8,128)(2,1)} %all-gather.2.cloned.1.call-done, bf16[3072,384]{1,0:T(8,128)(2,1)} %param.25), kind=kOutput, calls=%fused_computation.4 | convolution fusion | flops 1511915520 | bytes 9142272 | tf_op jit(solution)/shard_map/dot_general | solution.py:227
  121.1 46.8 %all_to_all.20 = bf16[8,40,3072]{2,1,0:T(8,128)(2,1)S(1)} all-to-all(bf16[8,40,3072]{2,1,0:T(8,128)(2,1)} %bitcast.92), channel_id=1, replica_groups=mesh['sp'=12,'tp'=8,'dp'=8] {'tp'}, dimensions={0} | all-to-all | bytes 3932160 | tf_op jit(solution)/shard_map/all_to_all | solution.py:57
  (61 shorter events, 11.7 us)
Async XLA Ops:
  6.5 108.6 %copy-start = (bf16[384,3072]{1,0:T(8,128)(2,1)S(1)}, bf16[384,3072]{1,0:T(8,128)(2,1)}, u32[]{:S(2)}) copy-start(bf16[384,3072]{1,0:T(8,128)(2,1)} %param.26) | copy-start | bytes 7077892
  6.5 48.4 %copy-start.5 = (bf16[32,3072]{1,0:T(8,128)(2,1)S(1)}, bf16[32,3072]{1,0:T(8,128)(2,1)}, u32[]{:S(2)}) copy-start(bf16[32,3072]{1,0:T(8,128)(2,1)} %param.17) | copy-start | bytes 589828
  6.5 48.9 %copy-start.4 = (bf16[3072,64]{0,1:T(8,128)(2,1)S(1)}, bf16[3072,64]{0,1:T(8,128)(2,1)}, u32[]{:S(2)}) copy-start(bf16[3072,64]{0,1:T(8,128)(2,1)} %param.24) | copy-start | bytes 1179652
  6.5 49.9 %copy-start.3 = (bf16[3072,64]{0,1:T(8,128)(2,1)S(1)}, bf16[3072,64]{0,1:T(8,128)(2,1)}, u32[]{:S(2)}) copy-start(bf16[3072,64]{0,1:T(8,128)(2,1)} %param.23) | copy-start | bytes 1179652
  11.5 22.8 %all-to-all-start = ((f32[12,5,384]{2,1,0:T(8,128)}), f32[12,5,384]{2,1,0:T(8,128)S(1)}, u32[]{:S(2)}, u32[]{:S(2)}) async-start(f32[12,5,384]{2,1,0:T(8,128)} %broadcast_in_dim.12), calls=%async_computation | async-start | bytes 294912 | tf_op jit(solution)/shard_map/all_to_all | solution.py:19
  35.0 15.8 %all-to-all-start.1 = ((f32[8,5,384]{2,1,0:T(8,128)}), f32[8,5,384]{2,1,0:T(8,128)S(1)}, u32[]{:S(2)}, u32[]{:S(2)}) async-start(f32[8,5,384]{2,1,0:T(8,128)} %broadcast_in_dim.13), calls=%async_computation.1 | async-start | bytes 196608 | tf_op jit(solution)/shard_map/all_to_all | solution.py:19
  42.1 49.4 %all-gather.2.cloned.1.call-start = ((), (), s32[]{:S(2)}) async-start(), calls=%async_computation.4 | async-start | bytes 2211840 | tf_op jit(solution)/shard_map/all_gather | solution.py:195
  58.2 46.2 %all-to-all-start.2 = ((bf16[12,32,128]{2,1,0:T(8,128)(2,1)}), bf16[12,32,128]{2,1,0:T(8,128)(2,1)S(1)}, u32[]{:S(2)}, u32[]{:S(2)}) async-start(bf16[12,32,128]{2,1,0:T(8,128)(2,1)} %broadcast_in_dim.16), calls=%async_computation.2 | async-start | bytes 196608 | tf_op jit(solution)/shard_map/all_to_all | solution.py:19
  91.5 3.4 %copy-start.1 = (bf16[320,3072]{1,0:T(8,128)(2,1)S(1)}, bf16[320,3072]{1,0:T(8,128)(2,1)}, u32[]{:S(2)}) copy-start(bf16[320,3072]{1,0:T(8,128)(2,1)} %all-gather.2.cloned.1.call-done) | copy-start | bytes 5898244
  91.5 11.3 %copy-start.10 = (bf16[3072,384]{1,0:T(8,128)(2,1)S(1)}, bf16[3072,384]{1,0:T(8,128)(2,1)}, u32[]{:S(2)}) copy-start(bf16[3072,384]{1,0:T(8,128)(2,1)} %param.22) | copy-start | bytes 7077892
  95.8 9.5 %collective-permute-start = (bf16[128,128]{0,1:T(8,128)(2,1)S(1)}, bf16[128,128]{0,1:T(8,128)(2,1)S(1)}, u32[]{:S(2)}, u32[]{:S(2)}) collective-permute-start(bf16[128,128]{0,1:T(8,128)(2,1)S(1)} %get-tuple-element.14), channel_id=1, source_target_pairs={{0,64},{64,128},{128,192},{192,256},{256,320},{320,384},{384,448},... | collective-permute-start | bytes 98312 | tf_op jit(solution)/shard_map/ppermute | solution.py:42
  100.6 3.7 %copy-start.6 = (f32[320,32]{0,1:T(8,128)S(1)}, f32[320,32]{0,1:T(8,128)}, u32[]{:S(2)}) copy-start(f32[320,32]{0,1:T(8,128)} %get-tuple-element.16) | copy-start | bytes 122884
  100.6 3.7 %copy-start.7 = (f32[320,32]{0,1:T(8,128)S(1)}, f32[320,32]{0,1:T(8,128)}, u32[]{:S(2)}) copy-start(f32[320,32]{0,1:T(8,128)} %get-tuple-element.17) | copy-start | bytes 122884
  100.6 7.2 %collective-permute-start.1 = (bf16[128,128]{0,1:T(8,128)(2,1)S(1)}, bf16[128,128]{0,1:T(8,128)(2,1)S(1)}, u32[]{:S(2)}, u32[]{:S(2)}) collective-permute-start(bf16[128,128]{0,1:T(8,128)(2,1)S(1)} %get-tuple-element.15), channel_id=1, source_target_pairs={{64,0},{128,64},{192,128},{256,192},{320,256},{384,320},{448,384},... | collective-permute-start | bytes 98312 | tf_op jit(solution)/shard_map/ppermute | solution.py:45
  105.2 3.9 %copy-start.9 = (f32[6]{0:T(128)S(1)}, f32[6]{0:T(128)}, u32[]{:S(2)}) copy-start(f32[6]{0:T(128)} %param.27) | copy-start | bytes 76
  121.1 47.1 %copy-start.2 = (bf16[40,3072]{1,0:T(8,128)(2,1)S(1)}, bf16[40,3072]{1,0:T(8,128)(2,1)}, u32[]{:S(2)}) copy-start(bf16[40,3072]{1,0:T(8,128)(2,1)} %param.14) | copy-start | bytes 737284
  121.1 47.1 %copy-start.8 = (f32[1,8,384]{2,0,1:T(1,128)S(1)}, f32[1,8,384]{2,0,1:T(1,128)}, u32[]{:S(2)}) copy-start(f32[1,8,384]{2,0,1:T(1,128)} %get-tuple-element.9) | copy-start | bytes 36868
Sparse Core Ops, SparseCore 0:
  53.4 38.0 all-gather.1
where the time goes:
time: 177 us; the launch traced here: 176 us
  waiting for transfers between devices  46.8 us (26%)
  blocking collectives  46.8 us (26%)
  starting transfers between devices  33.5 us (19%)
  matrix products  20.6 us (12%)
  between operations  13.7 us (8%)
  other arithmetic  11.2 us (6%)
  local copies, waits for them, and re-layouts  3.07 us (2%)
    all_to_all x1, blocking collectives, sum_at_owner(): tiles = lax.all_to_all(cut_along(shard, dim, size), axis, 0, 0, tiled=True)  46.8 us
    all_gather x1, waiting for transfers between devices, shards(): row_piece = lax.all_gather(hidden, 'tp', axis=0, tiled=True)  26.9 us
    all_to_all x3, starting transfers between devices, copy_for_each(): return lax.all_to_all(copies, axis, split_axis=0, concat_axis=0, tiled=True)  26.5 us
    all_to_all x3, waiting for transfers between devices, copy_for_each(): return lax.all_to_all(copies, axis, split_axis=0, concat_axis=0, tiled=True)  17.4 us
    dot_general x1, matrix products, shards(): jnp.dot(mixed, w_out, preferred_element_type=jnp.float32)  5.91 us
    ppermute x1, starting transfers between devices, with_halo(): lax.ppermute(lax.slice_in_dim(block, block.shape[dim] - width, None, axis...  4.81 us
  transfers between devices with their start and end apart: 6, of which 4 were waited for; matrix products, arithmetic and copies ran while one was open for 7% of the time, Pallas kernels for 0%

commit v1 on v0

--- a/solution.py
+++ b/solution.py
@@ -152,6 +152,7 @@
     w_out,
     sink_logit,
 ):
+    latent_rows = lax.all_gather(latent, "tp", axis=0, tiled=True)
     sp_count = lax.axis_size("sp")
     sp_rank = lax.axis_index("sp")
     mod_rows = mod_shift.shape[0]
@@ -176,7 +177,7 @@
     lat_scale = vectors[2]
     ctx_scale = vectors[3]
     lat_gate = vectors[4]
-    hidden = modulate(latent, norm_gain, lat_shift, lat_scale)
+    row_piece = modulate(latent_rows, norm_gain, lat_shift, lat_scale)
     ctx_hidden = modulate(context, norm_gain, ctx_shift, ctx_scale)
     kv_width = key_weight.shape[1]
     q_width = w_query.shape[1]
@@ -192,7 +193,6 @@
         axis=1,
     )
     ctx_all = gather_directly(ctx_pair, "sp", 0)
-    row_piece = lax.all_gather(hidden, "tp", axis=0, tiled=True)
     projected = jnp.concatenate(
         [
             jnp.dot(row_piece, w_query, preferred_element_type=jnp.float32),
@@ -223,9 +223,12 @@
         block_rows * sp_count,
     )
     mixed = (attended * jax.nn.silu(gate_proj.astype(jnp.float32))).astype(jnp.bfloat16)
-    branch = sum_at_owner(
-        jnp.dot(mixed, w_out, preferred_element_type=jnp.float32).astype(jnp.bfloat16), "tp", 0
-    )
+    branch = lax.psum_scatter(
+        jnp.dot(mixed, w_out, preferred_element_type=jnp.float32).astype(jnp.bfloat16),
+        "tp",
+        scatter_dimension=0,
+        tiled=True,
+    ).astype(jnp.float32)
     return (latent.astype(jnp.float32) + lat_gate * branch).astype(jnp.bfloat16)
 
 

time: 177 us -> 148 us (0.84)
  the two profiles are of different devices: /device:TPU:196 before, /device:TPU:2 now
where the time goes in v1:
time: 148 us; the launch traced here: 147 us
  waiting for transfers between devices  69.7 us (47%)
  starting transfers between devices  31.3 us (21%)
  matrix products  18.5 us (12%)
  between operations  13.7 us (9%)
  other arithmetic  10.9 us (7%)
  local copies, waits for them, and re-layouts  3.05 us (2%)
    reduce_scatter x1, waiting for transfers between devices, shards(): lax.psum_scatter(jnp.dot(mixed, w_out, preferred_element_type=jnp.float32...  47.3 us
    all_to_all x3, starting transfers between devices, copy_for_each(): return lax.all_to_all(copies, axis, split_axis=0, concat_axis=0, tiled=True)  25.9 us
    all_to_all x3, waiting for transfers between devices, copy_for_each(): return lax.all_to_all(copies, axis, split_axis=0, concat_axis=0, tiled=True)  19.7 us
    dot_general x1, matrix products, shards(): jnp.dot(mixed, w_out, preferred_element_type=jnp.float32)  5.97 us
    ppermute x1, starting transfers between devices, with_halo(): lax.ppermute(lax.slice_in_dim(block, block.shape[dim] - width, None, axis...  3.88 us
    reduce_sum x2, other arithmetic, modulate(): jnp.mean(values * values, axis=-1, keepdims=True) + NORM_EPS  3.25 us
  transfers between devices with their start and end apart: 7, of which 5 were waited for; matrix products, arithmetic and copies ran while one was open for 12% of the time, Pallas kernels for 0%

profile of v1, /device:TPU:2, one launch (start us, length us, event | category | flops | bytes accessed | tf_op | source)
XLA Modules:
  0.0 147.2 jit_solution(14514806074902729628)
XLA Ops:
  8.2 1.1 fusion.51
  9.2 1.1 fusion.46
  10.3 1.1 fusion.47
  12.1 15.2 %all-to-all-start = ((f32[12,5,384]{2,1,0:T(8,128)}), f32[12,5,384]{2,1,0:T(8,128)S(1)}, u32[]{:S(2)}, u32[]{:S(2)}) async-start(f32[12,5,384]{2,1,0:T(8,128)} %broadcast_in_dim.12), calls=%async_computation | async-start | bytes 294912 | tf_op jit(solution)/shard_map/all_to_all | solution.py:19
  27.3 1.1 fusion.19
  28.8 11.3 %all-to-all-done = f32[12,5,384]{2,1,0:T(8,128)S(1)} async-done(((f32[12,5,384]{2,1,0:T(8,128)}), f32[12,5,384]{2,1,0:T(8,128)S(1)}, u32[]{:S(2)}, u32[]{:S(2)}) %all-to-all-start) | async-done | bytes 92192 | tf_op jit(solution)/shard_map/all_to_all | solution.py:19
  40.7 7.1 %all-to-all-start.1 = ((f32[8,5,384]{2,1,0:T(8,128)}), f32[8,5,384]{2,1,0:T(8,128)S(1)}, u32[]{:S(2)}, u32[]{:S(2)}) async-start(f32[8,5,384]{2,1,0:T(8,128)} %broadcast_in_dim.13), calls=%async_computation.1 | async-start | bytes 196608 | tf_op jit(solution)/shard_map/all_to_all | solution.py:19
  48.0 8.4 %all-to-all-done.1 = f32[8,5,384]{2,1,0:T(8,128)S(1)} async-done(((f32[8,5,384]{2,1,0:T(8,128)}), f32[8,5,384]{2,1,0:T(8,128)S(1)}, u32[]{:S(2)}, u32[]{:S(2)}) %all-to-all-start.1) | async-done | bytes 61472 | tf_op jit(solution)/shard_map/all_to_all | solution.py:19
  57.0 1.4 convolution_convert_fusion.3
  59.5 3.7 %all-to-all-start.2 = ((bf16[12,32,128]{2,1,0:T(8,128)(2,1)}), bf16[12,32,128]{2,1,0:T(8,128)(2,1)S(1)}, u32[]{:S(2)}, u32[]{:S(2)}) async-start(bf16[12,32,128]{2,1,0:T(8,128)(2,1)} %broadcast_in_dim.16), calls=%async_computation.2 | async-start | bytes 196608 | tf_op jit(solution)/shard_map/all_to_all | solution.py:19
  63.4 2.2 %fusion.1 = f32[320]{0:T(512)S(1)} fusion(bf16[320,3072]{1,0:T(8,128)(2,1)} %all-gather.2.cloned.1.call-done), kind=kLoop, calls=%fused_computation.7 | loop fusion | flops 2948800 | bytes 1967360 | tf_op jit(solution)/shard_map/reduce_sum | solution.py:63
  65.6 0.9 fusion.5
  68.3 3.9 %collective-permute-start = (bf16[128,128]{0,1:T(8,128)(2,1)S(1)}, bf16[128,128]{0,1:T(8,128)(2,1)S(1)}, u32[]{:S(2)}, u32[]{:S(2)}) collective-permute-start(bf16[128,128]{0,1:T(8,128)(2,1)S(1)} %get-tuple-element.14), channel_id=1, source_target_pairs={{0,64},{64,128},{128,192},{192,256},{256,320},{320,384},{384,448},... | collective-permute-start | bytes 98312 | tf_op jit(solution)/shard_map/ppermute | solution.py:42
  72.2 1.5 %collective-permute-start.1 = (bf16[128,128]{0,1:T(8,128)(2,1)S(1)}, bf16[128,128]{0,1:T(8,128)(2,1)S(1)}, u32[]{:S(2)}, u32[]{:S(2)}) collective-permute-start(bf16[128,128]{0,1:T(8,128)(2,1)S(1)} %get-tuple-element.15), channel_id=1, source_target_pairs={{64,0},{128,64},{192,128},{256,192},{320,256},{384,320},{448,384},... | collective-permute-start | bytes 98312 | tf_op jit(solution)/shard_map/ppermute | solution.py:45
  73.7 1.5 fusion.52
  76.0 1.9 %collective-permute-done.1 = bf16[128,128]{0,1:T(8,128)(2,1)S(1)} collective-permute-done((bf16[128,128]{0,1:T(8,128)(2,1)S(1)}, bf16[128,128]{0,1:T(8,128)(2,1)S(1)}, u32[]{:S(2)}, u32[]{:S(2)}) %collective-permute-start.1) | collective-permute-done | bytes 32800 | tf_op jit(solution)/shard_map/ppermute | solution.py:45
  78.1 1.2 fusion.6
  80.3 1.3 fusion
  81.6 1.1 fusion.11
  82.8 1.6 %fusion.14 = f32[64,6,320]{2,0,1:T(8,128)S(1)} fusion(f32[64,6,320]{2,0,1:T(8,128)S(1)} %fusion.11, f32[6,320]{1,0:T(8,128)S(1)} %exponential_add_fusion, f32[6,320]{1,0:T(8,128)S(1)} %maximum_maximum_fusion, f32[576,320,6]{0,1,2:T(8,128)S(1)} %get-tuple-element.25, pred[320,576]{1,0:T(8,128)(4,1)S(1)} %fusion.18, bf16[576,128]{0,1:T(8,128)(2,1)S(1)} %pad_maximum_fusion.3), kind=kOutput, calls=%fused_computation.23 | convolution fusion | flops 147210240 | bytes 6307840 | tf_op jit(solution)/shard_map/kgqs,skd->qkgd/dot_general | solution.py:132
  84.4 1.0 copy.31
  85.4 6.0 %convolution_convert_fusion = bf16[320,3072]{1,0:T(8,128)(2,1)} fusion(bf16[384,3072]{1,0:T(8,128)(2,1)S(1)} %copy-done, f32[320,384]{1,0:T(8,128)} %copy.31, bf16[320,3072]{1,0:T(8,128)(2,1)} %copy-done.1, bf16[3072,384]{1,0:T(8,128)(2,1)} %param.25), kind=kOutput, calls=%fused_computation.6 | convolution fusion | flops 1511915520 | bytes 9142272 | tf_op jit(solution)/shard_map/dot_general | solution.py:227
  91.4 47.3 %reduce-scatter.2.cloned.1.call-done = bf16[40,3072]{1,0:T(8,128)(2,1)} async-done(((bf16[320,3072]{1,0:T(8,128)(2,1)}), bf16[40,3072]{1,0:T(8,128)(2,1)}) %reduce-scatter.2.cloned.1.call-update) | async-done | bytes 245776 | tf_op jit(solution)/shard_map/reduce_scatter | solution.py:226
  138.7 1.7 %add_convert_fusion = bf16[40,3072]{1,0:T(8,128)(2,1)} fusion(bf16[40,3072]{1,0:T(8,128)(2,1)} %reduce-scatter.2.cloned.1.call-done, bf16[40,3072]{1,0:T(8,128)(2,1)S(1)} %copy-done.3, f32[3072]{0:T(1024)S(1)} %bitcast.96), kind=kLoop, calls=%fused_computation.32 | loop fusion | flops 614400 | bytes 749568 | tf_op jit(solution)/shard_map/convert_element_type | solution.py:232
  (62 shorter events, 9.2 us)
Async XLA Ops:
  6.5 78.8 %copy-start = (bf16[384,3072]{1,0:T(8,128)(2,1)S(1)}, bf16[384,3072]{1,0:T(8,128)(2,1)}, u32[]{:S(2)}) copy-start(bf16[384,3072]{1,0:T(8,128)(2,1)} %param.26) | copy-start | bytes 7077892
  6.5 51.9 %copy-start.6 = (bf16[32,3072]{1,0:T(8,128)(2,1)S(1)}, bf16[32,3072]{1,0:T(8,128)(2,1)}, u32[]{:S(2)}) copy-start(bf16[32,3072]{1,0:T(8,128)(2,1)} %param.17) | copy-start | bytes 589828
  6.5 51.9 %copy-start.8 = (f32[3072]{0:T(1024)S(1)}, f32[3072]{0:T(1024)}, u32[]{:S(2)}) copy-start(f32[3072]{0:T(1024)} %param.21) | copy-start | bytes 36868
  6.5 52.0 %copy-start.5 = (bf16[3072,64]{0,1:T(8,128)(2,1)S(1)}, bf16[3072,64]{0,1:T(8,128)(2,1)}, u32[]{:S(2)}) copy-start(bf16[3072,64]{0,1:T(8,128)(2,1)} %param.23) | copy-start | bytes 1179652
  6.5 56.8 %all-gather.2.cloned.1.call-start = ((), (), s32[]{:S(2)}) async-start(), calls=%async_computation.4 | async-start | bytes 2211840 | tf_op jit(solution)/shard_map/all_gather | solution.py:155
  12.1 28.0 %all-to-all-start = ((f32[12,5,384]{2,1,0:T(8,128)}), f32[12,5,384]{2,1,0:T(8,128)S(1)}, u32[]{:S(2)}, u32[]{:S(2)}) async-start(f32[12,5,384]{2,1,0:T(8,128)} %broadcast_in_dim.12), calls=%async_computation | async-start | bytes 294912 | tf_op jit(solution)/shard_map/all_to_all | solution.py:19
  40.7 15.7 %all-to-all-start.1 = ((f32[8,5,384]{2,1,0:T(8,128)}), f32[8,5,384]{2,1,0:T(8,128)S(1)}, u32[]{:S(2)}, u32[]{:S(2)}) async-start(f32[8,5,384]{2,1,0:T(8,128)} %broadcast_in_dim.13), calls=%async_computation.1 | async-start | bytes 196608 | tf_op jit(solution)/shard_map/all_to_all | solution.py:19
  59.5 15.7 %all-to-all-start.2 = ((bf16[12,32,128]{2,1,0:T(8,128)(2,1)}), bf16[12,32,128]{2,1,0:T(8,128)(2,1)S(1)}, u32[]{:S(2)}, u32[]{:S(2)}) async-start(bf16[12,32,128]{2,1,0:T(8,128)(2,1)} %broadcast_in_dim.16), calls=%async_computation.2 | async-start | bytes 196608 | tf_op jit(solution)/shard_map/all_to_all | solution.py:19
  63.2 75.4 %reduce-scatter.2.cloned.1.call-start = ((), (), s32[]{:S(2)}) async-start(), calls=%async_computation.5 | async-start | bytes 2211840 | tf_op jit(solution)/shard_map/reduce_scatter | solution.py:226
  63.4 2.2 %copy-start.2 = (bf16[320,3072]{1,0:T(8,128)(2,1)S(1)}, bf16[320,3072]{1,0:T(8,128)(2,1)}, u32[]{:S(2)}) copy-start(bf16[320,3072]{1,0:T(8,128)(2,1)} %all-gather.2.cloned.1.call-done) | copy-start | bytes 5898244
  63.4 3.1 %copy-start.4 = (bf16[3072,64]{0,1:T(8,128)(2,1)S(1)}, bf16[3072,64]{0,1:T(8,128)(2,1)}, u32[]{:S(2)}) copy-start(bf16[3072,64]{0,1:T(8,128)(2,1)} %param.24) | copy-start | bytes 1179652
  66.5 7.2 %copy-start.1 = (bf16[320,3072]{1,0:T(8,128)(2,1)}, bf16[320,3072]{1,0:T(8,128)(2,1)S(1)}, u32[]{:S(2)}) copy-start(bf16[320,3072]{1,0:T(8,128)(2,1)S(1)} %fusion.5) | copy-start | bytes 5898244
  67.2 6.4 %copy-start.10 = (bf16[3072,384]{1,0:T(8,128)(2,1)S(1)}, bf16[3072,384]{1,0:T(8,128)(2,1)}, u32[]{:S(2)}) copy-start(bf16[3072,384]{1,0:T(8,128)(2,1)} %param.22) | copy-start | bytes 7077892
  68.3 7.7 %collective-permute-start = (bf16[128,128]{0,1:T(8,128)(2,1)S(1)}, bf16[128,128]{0,1:T(8,128)(2,1)S(1)}, u32[]{:S(2)}, u32[]{:S(2)}) collective-permute-start(bf16[128,128]{0,1:T(8,128)(2,1)S(1)} %get-tuple-element.14), channel_id=1, source_target_pairs={{0,64},{64,128},{128,192},{192,256},{256,320},{320,384},{384,448},... | collective-permute-start | bytes 98312 | tf_op jit(solution)/shard_map/ppermute | solution.py:42
  72.2 5.8 %collective-permute-start.1 = (bf16[128,128]{0,1:T(8,128)(2,1)S(1)}, bf16[128,128]{0,1:T(8,128)(2,1)S(1)}, u32[]{:S(2)}, u32[]{:S(2)}) collective-permute-start(bf16[128,128]{0,1:T(8,128)(2,1)S(1)} %get-tuple-element.15), channel_id=1, source_target_pairs={{64,0},{128,64},{192,128},{256,192},{320,256},{384,320},{448,384},... | collective-permute-start | bytes 98312 | tf_op jit(solution)/shard_map/ppermute | solution.py:45
  76.0 3.3 %copy-start.9 = (f32[6]{0:T(128)S(1)}, f32[6]{0:T(128)}, u32[]{:S(2)}) copy-start(f32[6]{0:T(128)} %param.27) | copy-start | bytes 76
  85.4 53.3 %copy-start.3 = (bf16[40,3072]{1,0:T(8,128)(2,1)S(1)}, bf16[40,3072]{1,0:T(8,128)(2,1)}, u32[]{:S(2)}) copy-start(bf16[40,3072]{1,0:T(8,128)(2,1)} %param.14) | copy-start | bytes 737284
  85.4 53.3 %copy-start.7 = (f32[1,8,384]{2,0,1:T(1,128)S(1)}, f32[1,8,384]{2,0,1:T(1,128)}, u32[]{:S(2)}) copy-start(f32[1,8,384]{2,0,1:T(1,128)} %get-tuple-element.9) | copy-start | bytes 36868
Sparse Core Ops, SparseCore 0:
  9.7 53.5 all-gather.1
  91.5 47.1 reduce-scatter.1

commit v2 on v0

--- a/solution.py
+++ b/solution.py
@@ -17,11 +17,6 @@
 def copy_for_each(shard, axis):
     copies = jnp.broadcast_to(shard, (lax.axis_size(axis), *shard.shape))
     return lax.all_to_all(copies, axis, split_axis=0, concat_axis=0, tiled=True)
-
-
-def taken_together(shard, axis):
-    everything = copy_for_each(shard, axis)
-    return jnp.sum(everything, axis=0)
 
 
 def laid_out(tiles, dim):
@@ -45,17 +40,6 @@
         high = lax.ppermute(lax.slice_in_dim(block, 0, width, axis=dim), axis, backward)
         block = jnp.concatenate([low, block, high], axis=dim)
     return block
-
-
-def cut_along(shard, dim, size):
-    before, after = (shard.shape[:dim], shard.shape[dim + 1 :])
-    return jnp.moveaxis(shard.reshape(*before, size, -1, *after), dim, 0)
-
-
-def sum_at_owner(shard, axis, dim):
-    size = lax.axis_size(axis)
-    tiles = lax.all_to_all(cut_along(shard, dim, size), axis, 0, 0, tiled=True)
-    return jnp.sum(tiles.astype(jnp.float32), axis=0)
 
 
 def modulate(row_data, gain_vec, shift_vec, scale_vec):
@@ -86,7 +70,7 @@
 
 
 def attend(
-    queries, key_rows, value_rows, ctx_keys, ctx_values, sink_logit, q_begin, k_begin, seq_total
+    queries, key_rows, value_rows, ctx_keys, ctx_values, sink_logit, q_pos, k_begin, seq_total
 ):
     row_count = queries.shape[0]
     key_count = key_rows.shape[0]
@@ -103,7 +87,6 @@
     near_scores = (
         jnp.einsum("qkgd,skd->kgqs", q_heads, k_heads, preferred_element_type=jnp.float32) * factor
     )
-    q_pos = q_begin + jnp.arange(row_count, dtype=jnp.int32)
     k_pos = k_begin + jnp.arange(key_count, dtype=jnp.int32)
     in_window = (jnp.abs(q_pos[:, None] - k_pos[None, :]) <= WINDOW) & (
         (k_pos >= 0) & (k_pos < seq_total)
@@ -136,7 +119,44 @@
     return result.reshape(row_count, head_count * HEAD_SIZE)
 
 
-def shards(
+def shift(block, steps):
+    count = lax.axis_size("tp")
+    return lax.ppermute(block, "tp", [(i, (i + steps) % count) for i in range(count)])
+
+
+def added(first, *others):
+    total = first.astype(jnp.float32)
+    for other in others:
+        total = total + other.astype(jnp.float32)
+    return total.astype(jnp.bfloat16)
+
+
+def gather_rows(latent):
+    half = latent.shape[1] // 2
+    low2, high2 = shift(latent, 2), shift(latent, -2)
+    low1, high1 = shift(latent, 1), shift(latent, -1)
+    low3, high3 = shift(low2, 1), shift(high2, -1)
+    far = jnp.concatenate([shift(low2[:, :half], 2), shift(high2[:, half:], -2)], axis=1)
+    return [low3, low2, low1, latent, high1, high2, high3, far]
+
+
+def reduce_rows(block):
+    half = block(0).shape[1] // 2
+    up3, down3 = shift(block(3), 1), shift(block(-3), -1)
+    far = block(4)
+    up4, down4 = shift(far[:, :half], 2), shift(far[:, half:], -2)
+    up1, down1 = shift(block(1), 1), shift(block(-1), -1)
+    gap = jnp.zeros_like(up4)
+    two = added(block(2), up3, jnp.concatenate([up4, gap], axis=1))
+    minus_two = added(block(-2), down3, jnp.concatenate([gap, down4], axis=1))
+    up2, down2 = shift(two, 2), shift(minus_two, -2)
+    total = block(0).astype(jnp.float32)
+    for part in (up1, down1, up2, down2):
+        total = total + part.astype(jnp.float32)
+    return total
+
+
+def body(
     latent,
     condition,
     ctx_condition,
@@ -152,6 +172,11 @@
     w_out,
     sink_logit,
 ):
+    tp_rank = lax.axis_index("tp")
+    tp_count = lax.axis_size("tp")
+    own_rows = latent.shape[0]
+    pieces = gather_rows(latent)
+    latent_rows = jnp.concatenate(pieces, axis=0)
     sp_count = lax.axis_size("sp")
     sp_rank = lax.axis_index("sp")
     mod_rows = mod_shift.shape[0]
@@ -169,14 +194,16 @@
         ],
         axis=0,
     )
-    summed = taken_together(partial_value, "sp")
-    vectors = gather_directly(summed, "tp", 1)
+    copies = copy_for_each(partial_value, "sp")
+    summed = jnp.sum(copies, axis=0)
+    vectors = copy_for_each(summed, "tp")
+    vectors = laid_out(vectors, 1)
     lat_shift = vectors[0]
     ctx_shift = vectors[1]
     lat_scale = vectors[2]
     ctx_scale = vectors[3]
     lat_gate = vectors[4]
-    hidden = modulate(latent, norm_gain, lat_shift, lat_scale)
+    row_piece = modulate(latent_rows, norm_gain, lat_shift, lat_scale)
     ctx_hidden = modulate(context, norm_gain, ctx_shift, ctx_scale)
     kv_width = key_weight.shape[1]
     q_width = w_query.shape[1]
@@ -192,7 +219,6 @@
         axis=1,
     )
     ctx_all = gather_directly(ctx_pair, "sp", 0)
-    row_piece = lax.all_gather(hidden, "tp", axis=0, tiled=True)
     projected = jnp.concatenate(
         [
             jnp.dot(row_piece, w_query, preferred_element_type=jnp.float32),
@@ -204,12 +230,20 @@
     )
     block_rows = projected.shape[0]
     q_begin = sp_rank * block_rows
-    positions = q_begin + jnp.arange(block_rows, dtype=jnp.int32)
+    local = jnp.arange(block_rows, dtype=jnp.int32)
+    place = (tp_rank + tp_count - 3) * own_rows + local
+    positions = q_begin + place % block_rows
     queries = rotate(projected[:, :q_width], positions).astype(jnp.bfloat16)
     key_rows = rotate(projected[:, q_width : q_width + kv_width], positions).astype(jnp.bfloat16)
     value_rows = projected[:, q_width + kv_width : q_width + 2 * kv_width].astype(jnp.bfloat16)
     gate_proj = projected[:, q_width + 2 * kv_width :].astype(jnp.bfloat16)
     key_value = jnp.concatenate([key_rows, value_rows], axis=1)
+    key_value = lax.dynamic_slice_in_dim(
+        jnp.concatenate([key_value, key_value], axis=0),
+        (tp_count + 3 - tp_rank) % tp_count * own_rows,
+        block_rows,
+        0,
+    )
     padded = with_halo(key_value, (("sp", 0),), WINDOW)
     attended = attend(
         queries,
@@ -218,20 +252,19 @@
         ctx_all[:, :kv_width],
         ctx_all[:, kv_width:],
         sink_logit,
-        q_begin,
+        positions,
         q_begin - WINDOW,
         block_rows * sp_count,
     )
     mixed = (attended * jax.nn.silu(gate_proj.astype(jnp.float32))).astype(jnp.bfloat16)
-    branch = sum_at_owner(
-        jnp.dot(mixed, w_out, preferred_element_type=jnp.float32).astype(jnp.bfloat16), "tp", 0
-    )
+    product = jnp.dot(mixed, w_out, preferred_element_type=jnp.float32).astype(jnp.bfloat16)
+    branch = reduce_rows(lambda d: product[(d + 3) * own_rows : (d + 4) * own_rows])
     return (latent.astype(jnp.float32) + lat_gate * branch).astype(jnp.bfloat16)
 
 
 def solution(mesh):
     return jax.shard_map(
-        shards,
+        body,
         mesh=mesh,
         in_specs=(
             P(("dp", "sp", "tp"), None),

time: 177 us -> 161 us (0.910)
  the two profiles are of different devices: /device:TPU:196 before, /device:TPU:6 now
where the time goes in v2:
time: 161 us; the launch traced here: 160 us
  starting transfers between devices  89.6 us (56%)
  waiting for transfers between devices  23.6 us (15%)
  matrix products  21.7 us (13%)
  other arithmetic  13.4 us (8%)
  local copies, waits for them, and re-layouts  11 us (7%)
    ppermute x16, starting transfers between devices, shift(): lax.ppermute(block, 'tp', [(i, (i + steps) % count) for i in range(count)])  60 us
    all_to_all x3, starting transfers between devices, copy_for_each(): return lax.all_to_all(copies, axis, split_axis=0, concat_axis=0, tiled=True)  24.4 us
    ppermute x16, waiting for transfers between devices, shift(): lax.ppermute(block, 'tp', [(i, (i + steps) % count) for i in range(count)])  11.1 us
    all_to_all x3, waiting for transfers between devices, copy_for_each(): return lax.all_to_all(copies, axis, split_axis=0, concat_axis=0, tiled=True)  9.74 us
    dot_general x1, matrix products, body(): jnp.dot(mixed, w_out, preferred_element_type=jnp.float32)  5.92 us
    unnamed x35, local copies, waits for them, and re-layouts  4.24 us
    ppermute x1, starting transfers between devices, with_halo(): lax.ppermute(lax.slice_in_dim(block, block.shape[dim] - width, None, axis...  3.77 us
    dot_general x1, matrix products, attend(): jnp.einsum('qkgd,skd->kgqs', q_heads, k_heads, preferred_element_type=jnp...  3.29 us
  transfers between devices with their start and end apart: 21, of which 6 were waited for; matrix products, arithmetic and copies ran while one was open for 18% of the time, Pallas kernels for 0%

profile of v2, /device:TPU:6, one launch (start us, length us, event | category | flops | bytes accessed | tf_op | source)
XLA Modules:
  0.0 160.0 jit_solution(17933681738694947187)
XLA Ops:
  0.0 5.5 %collective-permute-start.3 = (bf16[40,3072]{1,0:T(8,128)(2,1)}, bf16[40,3072]{1,0:T(8,128)(2,1)}, u32[]{:S(2)}, u32[]{:S(2)}) collective-permute-start(bf16[40,3072]{1,0:T(8,128)(2,1)} %param.14), channel_id=1, source_target_pairs={{0,56},{8,0},{16,8},{24,16},{32,24},{40,32},{48,40},{56,48},{1,57}... | collective-permute-start | bytes 737288 | tf_op jit(solution)/shard_map/ppermute | solution.py:124
  7.4 3.0 %collective-permute-start = (bf16[40,3072]{1,0:T(8,128)(2,1)}, bf16[40,3072]{1,0:T(8,128)(2,1)S(1)}, u32[]{:S(2)}, u32[]{:S(2)}) collective-permute-start(bf16[40,3072]{1,0:T(8,128)(2,1)} %param.14), channel_id=1, source_target_pairs={{0,16},{8,24},{16,32},{24,40},{32,48},{40,56},{48,0},{56,8},{1,17}... | collective-permute-start | bytes 737288 | tf_op jit(solution)/shard_map/ppermute | solution.py:124
  10.5 4.9 %collective-permute-start.4 = (bf16[40,3072]{1,0:T(8,128)(2,1)}, bf16[40,3072]{1,0:T(8,128)(2,1)S(1)}, u32[]{:S(2)}, u32[]{:S(2)}) collective-permute-start(bf16[40,3072]{1,0:T(8,128)(2,1)} %param.14), channel_id=1, source_target_pairs={{0,48},{8,56},{16,0},{24,8},{32,16},{40,24},{48,32},{56,40},{1,49}... | collective-permute-start | bytes 737288 | tf_op jit(solution)/shard_map/ppermute | solution.py:124
  20.2 15.2 %all-to-all-start = ((f32[12,5,384]{2,1,0:T(8,128)}), f32[12,5,384]{2,1,0:T(8,128)S(1)}, u32[]{:S(2)}, u32[]{:S(2)}) async-start(f32[12,5,384]{2,1,0:T(8,128)} %broadcast_in_dim.12), calls=%async_computation | async-start | bytes 294912 | tf_op jit(solution)/shard_map/all_to_all | solution.py:19
  37.6 9.7 %all-to-all-done = f32[12,5,384]{2,1,0:T(8,128)S(1)} async-done(((f32[12,5,384]{2,1,0:T(8,128)}), f32[12,5,384]{2,1,0:T(8,128)S(1)}, u32[]{:S(2)}, u32[]{:S(2)}) %all-to-all-start) | async-done | bytes 92192 | tf_op jit(solution)/shard_map/all_to_all | solution.py:19
  48.0 5.7 %all-to-all-start.1 = ((f32[8,5,384]{2,1,0:T(8,128)}), f32[8,5,384]{2,1,0:T(8,128)S(1)}, u32[]{:S(2)}, u32[]{:S(2)}) async-start(f32[8,5,384]{2,1,0:T(8,128)} %broadcast_in_dim.13), calls=%async_computation.1 | async-start | bytes 196608 | tf_op jit(solution)/shard_map/all_to_all | solution.py:19
  55.3 4.8 %collective-permute-start.6 = (bf16[40,1536]{1,0:T(8,128)(2,1)}, bf16[40,1536]{1,0:T(8,128)(2,1)}, u32[]{:S(2)}, u32[]{:S(2)}) collective-permute-start(bf16[40,1536]{1,0:T(8,128)(2,1)} %slice.113), channel_id=1, source_target_pairs={{0,16},{8,24},{16,32},{24,40},{32,48},{40,56},{48,0},{56,8},{1,17}... | collective-permute-start | bytes 368648 | tf_op jit(solution)/shard_map/ppermute | solution.py:124
  60.8 3.1 %collective-permute-start.7 = (bf16[40,1536]{1,0:T(8,128)(2,1)}, bf16[40,1536]{1,0:T(8,128)(2,1)}, u32[]{:S(2)}, u32[]{:S(2)}) collective-permute-start(bf16[40,1536]{1,0:T(8,128)(2,1)} %slice.114), channel_id=1, source_target_pairs={{0,48},{8,56},{16,0},{24,8},{32,16},{40,24},{48,32},{56,40},{1,49}... | collective-permute-start | bytes 368648 | tf_op jit(solution)/shard_map/ppermute | solution.py:124
  63.9 3.9 %collective-permute-start.1 = (bf16[40,3072]{1,0:T(8,128)(2,1)S(1)}, bf16[40,3072]{1,0:T(8,128)(2,1)}, u32[]{:S(2)}, u32[]{:S(2)}) collective-permute-start(bf16[40,3072]{1,0:T(8,128)(2,1)S(1)} %collective-permute-done), channel_id=1, source_target_pairs={{0,8},{8,16},{16,24},{24,32},{32,40},{40,48},{48,56},{56,0},{1,9},... | collective-permute-start | bytes 737288 | tf_op jit(solution)/shard_map/ppermute | solution.py:124
  72.1 3.5 %all-to-all-start.2 = ((bf16[12,32,128]{2,1,0:T(8,128)(2,1)}), bf16[12,32,128]{2,1,0:T(8,128)(2,1)S(1)}, u32[]{:S(2)}, u32[]{:S(2)}) async-start(bf16[12,32,128]{2,1,0:T(8,128)(2,1)} %broadcast_in_dim.16), calls=%async_computation.2 | async-start | bytes 196608 | tf_op jit(solution)/shard_map/all_to_all | solution.py:19
  75.6 3.1 %collective-permute-start.5 = (bf16[40,3072]{1,0:T(8,128)(2,1)S(1)}, bf16[40,3072]{1,0:T(8,128)(2,1)S(1)}, u32[]{:S(2)}, u32[]{:S(2)}) collective-permute-start(bf16[40,3072]{1,0:T(8,128)(2,1)S(1)} %collective-permute-done.4), channel_id=1, source_target_pairs={{0,56},{8,0},{16,8},{24,16},{32,24},{40,32},{48,40},{56,48},{1,57}... | collective-permute-start | bytes 737288 | tf_op jit(solution)/shard_map/ppermute | solution.py:124
  89.0 3.8 %collective-permute-start.8 = (bf16[128,128]{0,1:T(8,128)(2,1)S(1)}, bf16[128,128]{0,1:T(8,128)(2,1)S(1)}, u32[]{:S(2)}, u32[]{:S(2)}) collective-permute-start(bf16[128,128]{0,1:T(8,128)(2,1)S(1)} %get-tuple-element.22), channel_id=1, source_target_pairs={{0,64},{64,128},{128,192},{192,256},{256,320},{320,384},{384,448},... | collective-permute-start | bytes 98312 | tf_op jit(solution)/shard_map/ppermute | solution.py:37
  95.8 2.8 %collective-permute-done.9 = bf16[128,128]{0,1:T(8,128)(2,1)S(1)} collective-permute-done((bf16[128,128]{0,1:T(8,128)(2,1)S(1)}, bf16[128,128]{0,1:T(8,128)(2,1)S(1)}, u32[]{:S(2)}, u32[]{:S(2)}) %collective-permute-start.9) | collective-permute-done | bytes 32800 | tf_op jit(solution)/shard_map/ppermute | solution.py:40
  98.7 3.3 %fusion.6 = (f32[6,320]{1,0:T(8,128)S(1)}, f32[576,320,6]{0,1,2:T(8,128)}) fusion(pred[320,576]{1,0:T(8,128)(4,1)S(1)} %fusion.18, bf16[320,6,32]{0,2,1:T(8,128)(2,1)S(1)} %get-tuple-element.14, bf16[320,6,32]{0,2,1:T(8,128)(2,1)S(1)} %get-tuple-element.13, bf16[576,128]{0,1:T(8,128)(2,1)S(1)} %pad_maximum_fusion.3), kind=kOutput, calls=%fused_computation.12 | convolution fusion | flops 145365120 | bytes 5012992 | tf_op jit(solution)/shard_map/qkgd,skd->kgqs/dot_general | solution.py:88
  109.7 5.9 %convolution_convert_fusion = bf16[320,3072]{1,0:T(8,128)(2,1)} fusion(bf16[384,3072]{1,0:T(8,128)(2,1)S(1)} %copy-done, f32[320,384]{1,0:T(8,128)} %copy.31, bf16[320,3072]{1,0:T(8,128)(2,1)} %copy-done.1, bf16[3072,384]{1,0:T(8,128)(2,1)} %param.25), kind=kOutput, calls=%fused_computation.6 | convolution fusion | flops 1511915520 | bytes 9142272 | tf_op jit(solution)/shard_map/dot_general | solution.py:260
  117.0 4.3 %collective-permute-start.15 = (bf16[40,3072]{1,0:T(8,128)(2,1)S(1)}, bf16[40,3072]{1,0:T(8,128)(2,1)S(1)}, u32[]{:S(2)}, u32[]{:S(2)}) collective-permute-start(bf16[40,3072]{1,0:T(8,128)(2,1)S(1)} %get-tuple-element.6), channel_id=1, source_target_pairs={{0,56},{8,0},{16,8},{24,16},{32,24},{40,32},{48,40},{56,48},{1,57}... | collective-permute-start | bytes 737288 | tf_op jit(solution)/shard_map/ppermute | solution.py:124
  124.3 5.7 %collective-permute-start.13 = (bf16[40,1536]{1,0:T(8,128)(2,1)S(1)}, bf16[40,1536]{1,0:T(8,128)(2,1)S(1)}, u32[]{:S(2)}, u32[]{:S(2)}) collective-permute-start(bf16[40,1536]{1,0:T(8,128)(2,1)S(1)} %get-tuple-element.11), channel_id=1, source_target_pairs={{0,16},{8,24},{16,32},{24,40},{32,48},{40,56},{48,0},{56,8},{1,17}... | collective-permute-start | bytes 368648 | tf_op jit(solution)/shard_map/ppermute | solution.py:124
  130.0 2.2 %collective-permute-start.16 = (bf16[40,1536]{1,0:T(8,128)(2,1)S(1)}, bf16[40,1536]{1,0:T(8,128)(2,1)S(1)}, u32[]{:S(2)}, u32[]{:S(2)}) collective-permute-start(bf16[40,1536]{1,0:T(8,128)(2,1)S(1)} %get-tuple-element.12), channel_id=1, source_target_pairs={{0,48},{8,56},{16,0},{24,8},{32,16},{40,24},{48,32},{56,40},{1,49}... | collective-permute-start | bytes 368648 | tf_op jit(solution)/shard_map/ppermute | solution.py:124
  132.2 4.8 %collective-permute-start.10 = (bf16[40,3072]{1,0:T(8,128)(2,1)S(1)}, bf16[40,3072]{1,0:T(8,128)(2,1)S(1)}, u32[]{:S(2)}, u32[]{:S(2)}) collective-permute-start(bf16[40,3072]{1,0:T(8,128)(2,1)S(1)} %get-tuple-element.5), channel_id=1, source_target_pairs={{0,8},{8,16},{16,24},{24,32},{32,40},{40,48},{48,56},{56,0},{1,9},... | collective-permute-start | bytes 737288 | tf_op jit(solution)/shard_map/ppermute | solution.py:124
  137.1 2.6 %collective-permute-start.11 = (bf16[40,3072]{1,0:T(8,128)(2,1)S(1)}, bf16[40,3072]{1,0:T(8,128)(2,1)S(1)}, u32[]{:S(2)}, u32[]{:S(2)}) collective-permute-start(bf16[40,3072]{1,0:T(8,128)(2,1)S(1)} %get-tuple-element.8), channel_id=1, source_target_pairs={{0,56},{8,0},{16,8},{24,16},{32,24},{40,32},{48,40},{56,48},{1,57}... | collective-permute-start | bytes 737288 | tf_op jit(solution)/shard_map/ppermute | solution.py:124
  141.0 5.5 %collective-permute-start.14 = (bf16[40,3072]{1,0:T(8,128)(2,1)S(1)}, bf16[40,3072]{1,0:T(8,128)(2,1)S(1)}, u32[]{:S(2)}, u32[]{:S(2)}) collective-permute-start(bf16[40,3072]{1,0:T(8,128)(2,1)S(1)} %get-tuple-element.9), channel_id=1, source_target_pairs={{0,16},{8,24},{16,32},{24,40},{32,48},{40,56},{48,0},{56,8},{1,17}... | collective-permute-start | bytes 737288 | tf_op jit(solution)/shard_map/ppermute | solution.py:124
  146.6 2.4 %collective-permute-start.17 = (bf16[40,3072]{1,0:T(8,128)(2,1)S(1)}, bf16[40,3072]{1,0:T(8,128)(2,1)S(1)}, u32[]{:S(2)}, u32[]{:S(2)}) collective-permute-start(bf16[40,3072]{1,0:T(8,128)(2,1)S(1)} %get-tuple-element.10), channel_id=1, source_target_pairs={{0,48},{8,56},{16,0},{24,8},{32,16},{40,24},{48,32},{56,40},{1,49}... | collective-permute-start | bytes 737288 | tf_op jit(solution)/shard_map/ppermute | solution.py:124
  149.1 4.7 %collective-permute-done.14 = bf16[40,3072]{1,0:T(8,128)(2,1)S(1)} collective-permute-done((bf16[40,3072]{1,0:T(8,128)(2,1)S(1)}, bf16[40,3072]{1,0:T(8,128)(2,1)S(1)}, u32[]{:S(2)}, u32[]{:S(2)}) %collective-permute-start.14) | collective-permute-done | bytes 245792 | tf_op jit(solution)/shard_map/ppermute | solution.py:124
  153.8 4.3 %collective-permute-done.17 = bf16[40,3072]{1,0:T(8,128)(2,1)S(1)} collective-permute-done((bf16[40,3072]{1,0:T(8,128)(2,1)S(1)}, bf16[40,3072]{1,0:T(8,128)(2,1)S(1)}, u32[]{:S(2)}, u32[]{:S(2)}) %collective-permute-start.17) | collective-permute-done | bytes 245792 | tf_op jit(solution)/shard_map/ppermute | solution.py:124
  (108 shorter events, 44.3 us)
Async XLA Ops:
  0.0 109.7 %copy-start = (bf16[384,3072]{1,0:T(8,128)(2,1)S(1)}, bf16[384,3072]{1,0:T(8,128)(2,1)}, u32[]{:S(2)}) copy-start(bf16[384,3072]{1,0:T(8,128)(2,1)} %param.26) | copy-start | bytes 7077892
  0.0 80.8 %collective-permute-start.3 = (bf16[40,3072]{1,0:T(8,128)(2,1)}, bf16[40,3072]{1,0:T(8,128)(2,1)}, u32[]{:S(2)}, u32[]{:S(2)}) collective-permute-start(bf16[40,3072]{1,0:T(8,128)(2,1)} %param.14), channel_id=1, source_target_pairs={{0,56},{8,0},{16,8},{24,16},{32,24},{40,32},{48,40},{56,48},{1,57}... | collective-permute-start | bytes 737288 | tf_op jit(solution)/shard_map/ppermute | solution.py:124
  5.5 74.3 %collective-permute-start.2 = (bf16[40,3072]{1,0:T(8,128)(2,1)}, bf16[40,3072]{1,0:T(8,128)(2,1)}, u32[]{:S(2)}, u32[]{:S(2)}) collective-permute-start(bf16[40,3072]{1,0:T(8,128)(2,1)} %param.14), channel_id=1, source_target_pairs={{0,8},{8,16},{16,24},{24,32},{32,40},{40,48},{48,56},{56,0},{1,9},... | collective-permute-start | bytes 737288 | tf_op jit(solution)/shard_map/ppermute | solution.py:124
  7.4 47.2 %collective-permute-start = (bf16[40,3072]{1,0:T(8,128)(2,1)}, bf16[40,3072]{1,0:T(8,128)(2,1)S(1)}, u32[]{:S(2)}, u32[]{:S(2)}) collective-permute-start(bf16[40,3072]{1,0:T(8,128)(2,1)} %param.14), channel_id=1, source_target_pairs={{0,16},{8,24},{16,32},{24,40},{32,48},{40,56},{48,0},{56,8},{1,17}... | collective-permute-start | bytes 737288 | tf_op jit(solution)/shard_map/ppermute | solution.py:124
  10.5 49.6 %collective-permute-start.4 = (bf16[40,3072]{1,0:T(8,128)(2,1)}, bf16[40,3072]{1,0:T(8,128)(2,1)S(1)}, u32[]{:S(2)}, u32[]{:S(2)}) collective-permute-start(bf16[40,3072]{1,0:T(8,128)(2,1)} %param.14), channel_id=1, source_target_pairs={{0,48},{8,56},{16,0},{24,8},{32,16},{40,24},{48,32},{56,40},{1,49}... | collective-permute-start | bytes 737288 | tf_op jit(solution)/shard_map/ppermute | solution.py:124
  20.2 27.1 %all-to-all-start = ((f32[12,5,384]{2,1,0:T(8,128)}), f32[12,5,384]{2,1,0:T(8,128)S(1)}, u32[]{:S(2)}, u32[]{:S(2)}) async-start(f32[12,5,384]{2,1,0:T(8,128)} %broadcast_in_dim.12), calls=%async_computation | async-start | bytes 294912 | tf_op jit(solution)/shard_map/all_to_all | solution.py:19
  37.5 43.3 %copy-start.3 = (bf16[40,3072]{1,0:T(8,128)(2,1)S(1)}, bf16[40,3072]{1,0:T(8,128)(2,1)}, u32[]{:S(2)}) copy-start(bf16[40,3072]{1,0:T(8,128)(2,1)} %param.14) | copy-start | bytes 737284
  48.0 19.9 %all-to-all-start.1 = ((f32[8,5,384]{2,1,0:T(8,128)}), f32[8,5,384]{2,1,0:T(8,128)S(1)}, u32[]{:S(2)}, u32[]{:S(2)}) async-start(f32[8,5,384]{2,1,0:T(8,128)} %broadcast_in_dim.13), calls=%async_computation.1 | async-start | bytes 196608 | tf_op jit(solution)/shard_map/all_to_all | solution.py:19
  55.3 28.4 %collective-permute-start.6 = (bf16[40,1536]{1,0:T(8,128)(2,1)}, bf16[40,1536]{1,0:T(8,128)(2,1)}, u32[]{:S(2)}, u32[]{:S(2)}) collective-permute-start(bf16[40,1536]{1,0:T(8,128)(2,1)} %slice.113), channel_id=1, source_target_pairs={{0,16},{8,24},{16,32},{24,40},{32,48},{40,56},{48,0},{56,8},{1,17}... | collective-permute-start | bytes 368648 | tf_op jit(solution)/shard_map/ppermute | solution.py:124
  60.8 23.0 %collective-permute-start.7 = (bf16[40,1536]{1,0:T(8,128)(2,1)}, bf16[40,1536]{1,0:T(8,128)(2,1)}, u32[]{:S(2)}, u32[]{:S(2)}) collective-permute-start(bf16[40,1536]{1,0:T(8,128)(2,1)} %slice.114), channel_id=1, source_target_pairs={{0,48},{8,56},{16,0},{24,8},{32,16},{40,24},{48,32},{56,40},{1,49}... | collective-permute-start | bytes 368648 | tf_op jit(solution)/shard_map/ppermute | solution.py:124
  63.9 11.7 %collective-permute-start.1 = (bf16[40,3072]{1,0:T(8,128)(2,1)S(1)}, bf16[40,3072]{1,0:T(8,128)(2,1)}, u32[]{:S(2)}, u32[]{:S(2)}) collective-permute-start(bf16[40,3072]{1,0:T(8,128)(2,1)S(1)} %collective-permute-done), channel_id=1, source_target_pairs={{0,8},{8,16},{16,24},{24,32},{32,40},{40,48},{48,56},{56,0},{1,9},... | collective-permute-start | bytes 737288 | tf_op jit(solution)/shard_map/ppermute | solution.py:124
  72.1 29.9 %all-to-all-start.2 = ((bf16[12,32,128]{2,1,0:T(8,128)(2,1)}), bf16[12,32,128]{2,1,0:T(8,128)(2,1)S(1)}, u32[]{:S(2)}, u32[]{:S(2)}) async-start(bf16[12,32,128]{2,1,0:T(8,128)(2,1)} %broadcast_in_dim.16), calls=%async_computation.2 | async-start | bytes 196608 | tf_op jit(solution)/shard_map/all_to_all | solution.py:19
  75.6 8.1 %collective-permute-start.5 = (bf16[40,3072]{1,0:T(8,128)(2,1)S(1)}, bf16[40,3072]{1,0:T(8,128)(2,1)S(1)}, u32[]{:S(2)}, u32[]{:S(2)}) collective-permute-start(bf16[40,3072]{1,0:T(8,128)(2,1)S(1)} %collective-permute-done.4), channel_id=1, source_target_pairs={{0,56},{8,0},{16,8},{24,16},{32,24},{40,32},{48,40},{56,48},{1,57}... | collective-permute-start | bytes 737288 | tf_op jit(solution)/shard_map/ppermute | solution.py:124
  89.0 6.8 %collective-permute-start.8 = (bf16[128,128]{0,1:T(8,128)(2,1)S(1)}, bf16[128,128]{0,1:T(8,128)(2,1)S(1)}, u32[]{:S(2)}, u32[]{:S(2)}) collective-permute-start(bf16[128,128]{0,1:T(8,128)(2,1)S(1)} %get-tuple-element.22), channel_id=1, source_target_pairs={{0,64},{64,128},{128,192},{192,256},{256,320},{320,384},{384,448},... | collective-permute-start | bytes 98312 | tf_op jit(solution)/shard_map/ppermute | solution.py:37
  92.8 5.8 %collective-permute-start.9 = (bf16[128,128]{0,1:T(8,128)(2,1)S(1)}, bf16[128,128]{0,1:T(8,128)(2,1)S(1)}, u32[]{:S(2)}, u32[]{:S(2)}) collective-permute-start(bf16[128,128]{0,1:T(8,128)(2,1)S(1)} %get-tuple-element.23), channel_id=1, source_target_pairs={{64,0},{128,64},{192,128},{256,192},{320,256},{384,320},{448,384},... | collective-permute-start | bytes 98312 | tf_op jit(solution)/shard_map/ppermute | solution.py:40
  115.6 42.6 %copy-start.8 = (f32[1,8,384]{2,0,1:T(1,128)S(1)}, f32[1,8,384]{2,0,1:T(1,128)}, u32[]{:S(2)}) copy-start(f32[1,8,384]{2,0,1:T(1,128)} %get-tuple-element.17) | copy-start | bytes 36868
  117.0 22.7 %collective-permute-start.15 = (bf16[40,3072]{1,0:T(8,128)(2,1)S(1)}, bf16[40,3072]{1,0:T(8,128)(2,1)S(1)}, u32[]{:S(2)}, u32[]{:S(2)}) collective-permute-start(bf16[40,3072]{1,0:T(8,128)(2,1)S(1)} %get-tuple-element.6), channel_id=1, source_target_pairs={{0,56},{8,0},{16,8},{24,16},{32,24},{40,32},{48,40},{56,48},{1,57}... | collective-permute-start | bytes 737288 | tf_op jit(solution)/shard_map/ppermute | solution.py:124
  121.4 18.4 %collective-permute-start.12 = (bf16[40,3072]{1,0:T(8,128)(2,1)S(1)}, bf16[40,3072]{1,0:T(8,128)(2,1)S(1)}, u32[]{:S(2)}, u32[]{:S(2)}) collective-permute-start(bf16[40,3072]{1,0:T(8,128)(2,1)S(1)} %get-tuple-element.7), channel_id=1, source_target_pairs={{0,8},{8,16},{16,24},{24,32},{32,40},{40,48},{48,56},{56,0},{1,9},... | collective-permute-start | bytes 737288 | tf_op jit(solution)/shard_map/ppermute | solution.py:124
  124.3 12.8 %collective-permute-start.13 = (bf16[40,1536]{1,0:T(8,128)(2,1)S(1)}, bf16[40,1536]{1,0:T(8,128)(2,1)S(1)}, u32[]{:S(2)}, u32[]{:S(2)}) collective-permute-start(bf16[40,1536]{1,0:T(8,128)(2,1)S(1)} %get-tuple-element.11), channel_id=1, source_target_pairs={{0,16},{8,24},{16,32},{24,40},{32,48},{40,56},{48,0},{56,8},{1,17}... | collective-permute-start | bytes 368648 | tf_op jit(solution)/shard_map/ppermute | solution.py:124
  130.0 9.7 %collective-permute-start.16 = (bf16[40,1536]{1,0:T(8,128)(2,1)S(1)}, bf16[40,1536]{1,0:T(8,128)(2,1)S(1)}, u32[]{:S(2)}, u32[]{:S(2)}) collective-permute-start(bf16[40,1536]{1,0:T(8,128)(2,1)S(1)} %get-tuple-element.12), channel_id=1, source_target_pairs={{0,48},{8,56},{16,0},{24,8},{32,16},{40,24},{48,32},{56,40},{1,49}... | collective-permute-start | bytes 368648 | tf_op jit(solution)/shard_map/ppermute | solution.py:124
  132.2 16.7 %collective-permute-start.10 = (bf16[40,3072]{1,0:T(8,128)(2,1)S(1)}, bf16[40,3072]{1,0:T(8,128)(2,1)S(1)}, u32[]{:S(2)}, u32[]{:S(2)}) collective-permute-start(bf16[40,3072]{1,0:T(8,128)(2,1)S(1)} %get-tuple-element.5), channel_id=1, source_target_pairs={{0,8},{8,16},{16,24},{24,32},{32,40},{40,48},{48,56},{56,0},{1,9},... | collective-permute-start | bytes 737288 | tf_op jit(solution)/shard_map/ppermute | solution.py:124
  137.1 12.0 %collective-permute-start.11 = (bf16[40,3072]{1,0:T(8,128)(2,1)S(1)}, bf16[40,3072]{1,0:T(8,128)(2,1)S(1)}, u32[]{:S(2)}, u32[]{:S(2)}) collective-permute-start(bf16[40,3072]{1,0:T(8,128)(2,1)S(1)} %get-tuple-element.8), channel_id=1, source_target_pairs={{0,56},{8,0},{16,8},{24,16},{32,24},{40,32},{48,40},{56,48},{1,57}... | collective-permute-start | bytes 737288 | tf_op jit(solution)/shard_map/ppermute | solution.py:124
  141.0 12.8 %collective-permute-start.14 = (bf16[40,3072]{1,0:T(8,128)(2,1)S(1)}, bf16[40,3072]{1,0:T(8,128)(2,1)S(1)}, u32[]{:S(2)}, u32[]{:S(2)}) collective-permute-start(bf16[40,3072]{1,0:T(8,128)(2,1)S(1)} %get-tuple-element.9), channel_id=1, source_target_pairs={{0,16},{8,24},{16,32},{24,40},{32,48},{40,56},{48,0},{56,8},{1,17}... | collective-permute-start | bytes 737288 | tf_op jit(solution)/shard_map/ppermute | solution.py:124
  146.6 11.6 %collective-permute-start.17 = (bf16[40,3072]{1,0:T(8,128)(2,1)S(1)}, bf16[40,3072]{1,0:T(8,128)(2,1)S(1)}, u32[]{:S(2)}, u32[]{:S(2)}) collective-permute-start(bf16[40,3072]{1,0:T(8,128)(2,1)S(1)} %get-tuple-element.10), channel_id=1, source_target_pairs={{0,48},{8,56},{16,0},{24,8},{32,16},{40,24},{48,32},{56,40},{1,49}... | collective-permute-start | bytes 737288 | tf_op jit(solution)/shard_map/ppermute | solution.py:124
  (11 other events, 41.2 us)

commit v3 on v2

v3 whole, which is shorter than its diff:
```python
import functools
import math

import jax
import jax.numpy as jnp
from jax import lax
from jax.experimental import pallas as pl
from jax.experimental.pallas import tpu as pltpu
from jax.sharding import PartitionSpec as P

HEAD_SIZE = 64
WINDOW = 128
GRID_W = 64
LANES = 128
NORM_EPS = 1e-06
MASK_VALUE = -1e30
VMEM = pl.BlockSpec(memory_space=pltpu.VMEM)
ANY = pl.BlockSpec(memory_space=pl.ANY)
SMEM = pl.BlockSpec(memory_space=pltpu.SMEM)


def rounded(values):
    return values.astype(jnp.bfloat16)


def contract(left, right, right_dim=0):
    return lax.dot_general(
        left, right, (((1,), (right_dim,)), ((), ())), preferred_element_type=jnp.float32
    )


def call(kernel, out_shape, *operands, specs=None, scratch=(), flops=10**9):
    return pl.pallas_call(
        kernel,
        out_shape=out_shape,
        in_specs=specs or [VMEM] * len(operands),
        out_specs=jax.tree.map(lambda _: VMEM, out_shape),
        scratch_shapes=scratch,
        compiler_params=pltpu.CompilerParams(vmem_limit_bytes=VMEM_GRANT),
        cost_estimate=pl.CostEstimate(flops=flops, bytes_accessed=10**6, transcendentals=0),
    )(*operands)


VMEM_GRANT = 30 * 2**20


def partial_kernel(acts, shift, scale, gate, out):
    sums = jnp.concatenate(
        [
            contract(acts[...], shift[...]),
            contract(acts[...], scale[...]),
            contract(acts[...], gate[...])[:1],
        ],
        axis=0,
    )
    for copy in range(out.shape[0]):
        out[copy] = sums


def total_kernel(parts, out):
    total = parts[0]
    for index in range(1, parts.shape[0]):
        total = total + parts[index]
    for copy in range(out.shape[0]):
        out[copy] = total


def modulated(pieces, vectors, gain, shift_row, scale_row, store):
    blocks, _, width = vectors.shape
    for read in pieces:
        square = None
        for block in range(blocks):
            values = read(block * width, width)
            part = sum(
                values[:, lane : lane + LANES] * values[:, lane : lane + LANES]
                for lane in range(0, width, LANES)
            )
            square = part if square is None else square + part
        mean = jnp.sum(square, axis=1, keepdims=True) / (blocks * width)
        inverse = lax.rsqrt(mean + NORM_EPS)
        for block in range(blocks):
            values = read(block * width, width)
            factor = gain[:, block * width : (block + 1) * width] * (
                1.0 + vectors[block, scale_row : scale_row + 1, :]
            )
            moved = values * inverse * factor + vectors[block, shift_row : shift_row + 1, :]
            store(read, block * width, rounded(moved))


def context_kernel(context, vectors, gain, kv_weight, out, hidden):
    def store(_, column, rows):
        hidden[:, column : column + rows.shape[1]] = rows

    modulated([lambda c, n: context[:, c : c + n].astype(jnp.float32)], vectors, gain, 1, 3, store)
    pair = rounded(contract(hidden[...], kv_weight[...], 1))
    for copy in range(out.shape[0]):
        out[copy] = pair


def turned(values, cosine, sine):
    lane = lax.broadcasted_iota(jnp.int32, values.shape, 1)
    half = HEAD_SIZE // 2
    other = jnp.where(
        lane % HEAD_SIZE < half, pltpu.roll(values, LANES - half, 1), pltpu.roll(values, half, 1)
    )
    return values * cosine + other * sine


def key_kernel(*refs, pieces, per_group):
    count = sum(len(piece) for piece in pieces)
    place, *blocks = refs[: 1 + count]
    vectors, gain, kv_weight, cosine, sine = refs[1 + count : 6 + count]
    hidden, key_value, first, last, ordered = refs[6 + count :]
    own = hidden.shape[0] // len(pieces)
    members = [[blocks.pop(0) for _ in piece] for piece in pieces]
    reads, places = [], {}
    for group in range(0, len(members), per_group):

        def read(column, columns, parts=members[group : group + per_group]):
            rows = []
            for part in parts:
                held = part[0].shape[1]
                ref, at = part[column // held], column % held
                rows.append(ref[:, at : at + columns].astype(jnp.float32))
            return jnp.concatenate(rows, axis=0) if len(rows) > 1 else rows[0]

        reads.append(read)
        places[read] = group * own

    def store(read, column, rows):
        begin = places[read]
        hidden[begin : begin + rows.shape[0], column : column + rows.shape[1]] = rows

    modulated(reads, vectors, gain, 0, 2, store)
    both = contract(hidden[...], kv_weight[...], 1)
    lane = lax.broadcasted_iota(jnp.int32, both.shape, 1)
    both = jnp.where(lane < HEAD_SIZE, turned(both, cosine[...], sine[...]), both)
    for index in range(len(pieces)):
        begin = pl.multiple_of(place[2 + index], 8)
        ordered[pl.ds(begin, own), :] = both[index * own : (index + 1) * own, :]
    key_value[...] = rounded(ordered[...])
    first[...] = rounded(ordered[:WINDOW, :])
    last[...] = rounded(ordered[ordered.shape[0] - WINDOW :, :])


def query_kernel(hidden, w_query, w_gate, cosine, sine, queries, gate, held, ready, *, own):
    fetch = pltpu.make_async_copy(w_gate, held, ready)
    fetch.start()
    rows, width = hidden.shape[0], w_query.shape[1]
    projected = contract(hidden[...], w_query[...])
    heads = width // HEAD_SIZE
    lane = lax.broadcasted_iota(jnp.int32, (rows, LANES), 1)
    for pair in range(width // LANES):
        tile = turned(projected[:, pair * LANES : (pair + 1) * LANES], cosine[...], sine[...])
        tile = tile * (1.0 / math.sqrt(HEAD_SIZE))
        for odd in range(2):
            head = 2 * pair + odd
            aligned = pltpu.roll(tile, HEAD_SIZE, 1) if odd else tile
            aligned = jnp.where(lane < HEAD_SIZE, aligned, 0.0)
            for block in range(rows // own):
                begin = (block * heads + head) * own
                queries[begin : begin + own, :] = aligned[block * own : (block + 1) * own, :]
    fetch.wait()
    gate[...] = rounded(contract(hidden[...], held[...])).astype(jnp.float32)


def attend_kernel(
    place,
    sink,
    queries,
    gate,
    low,
    middle,
    high,
    ctx,
    w_out,
    out,
    padded,
    mixed,
    held,
    ready,
    *,
    own,
    span,
):
    fetch = pltpu.make_async_copy(w_out, held, ready)
    fetch.start()
    rows = middle.shape[0]
    width = w_out.shape[0]
    heads = width // HEAD_SIZE
    padded[:WINDOW, :] = low[...].astype(jnp.float32)
    padded[WINDOW : WINDOW + rows, :] = middle[...].astype(jnp.float32)
    padded[WINDOW + rows : 2 * WINDOW + rows, :] = high[...].astype(jnp.float32)
    padded[2 * WINDOW + rows :, :] = jnp.zeros_like(padded[2 * WINDOW + rows :, :])
    row = lax.broadcasted_iota(jnp.int32, (own, span), 0)
    column = lax.broadcasted_iota(jnp.int32, (own, span), 1)
    in_reach = (column >= row) & (column <= row + 2 * WINDOW)
    lane = lax.broadcasted_iota(jnp.int32, (own, LANES), 1)
    sinks = jnp.concatenate([jnp.full((own, 1), sink[h], jnp.float32) for h in range(heads)], axis=0)
    blocks = rows // own
    for block in range(blocks):
        offset = pl.multiple_of(place[2 + block], 8)
        near = rounded(padded[pl.ds(offset, span), :])
        query = rounded(queries[block * heads * own : (block + 1) * heads * own, :])
        near_scores = contract(query, near, 1)
        ctx_scores = contract(query, ctx[...], 1)
        token = place[0] - WINDOW + offset + column
        seen = in_reach & (token >= 0) & (token < place[1])
        near_scores = jnp.where(
            seen[None], near_scores.reshape(heads, own, span), MASK_VALUE
        ).reshape(heads * own, span)
        peak = jnp.maximum(
            jnp.maximum(
                jnp.max(near_scores, axis=1, keepdims=True),
                jnp.max(ctx_scores, axis=1, keepdims=True),
            ),
            sinks,
        )
        near_exp = jnp.exp(near_scores - peak)
        ctx_exp = jnp.exp(ctx_scores - peak)
        denominator = (
            jnp.sum(near_exp, axis=1, keepdims=True)
            + jnp.sum(ctx_exp, axis=1, keepdims=True)
            + jnp.exp(sinks - peak)
        )
        inverse = 1.0 / denominator
        result = contract(rounded(near_exp * inverse), near) + contract(
            rounded(ctx_exp * inverse), ctx[...]
        )
        here = slice(block * own, (block + 1) * own)
        for pair in range(heads // 2):
            even = result[2 * pair * own : (2 * pair + 1) * own, :]
            odd = result[(2 * pair + 1) * own : (2 * pair + 2) * own, :]
            attended = jnp.where(lane < HEAD_SIZE, pltpu.roll(even, HEAD_SIZE, 1), odd)
            tile = gate[here, pair * LANES : (pair + 1) * LANES]
            mixed[here, pair * LANES : (pair + 1) * LANES] = attended * (
                tile / (1.0 + jnp.exp(-tile))
            )
    fetch.wait()
    final = rounded(mixed[...])
    step = 512
    for begin in range(0, w_out.shape[1], step):
        out[:, begin : begin + step] = rounded(contract(final, held[:, begin : begin + step]))


def copy_for_each(copies, axis):
    return lax.all_to_all(copies, axis, split_axis=0, concat_axis=0, tiled=True)


def shift(block, axis, steps, wrap=True):
    count = lax.axis_size(axis)
    pairs = [(i, (i + steps) % count) for i in range(count) if wrap or 0 <= i + steps < count]
    return lax.ppermute(block, axis, pairs)


def added(first, *others):
    total = first.astype(jnp.float32)
    for other in others:
        total = total + other.astype(jnp.float32)
    return rounded(total)


def gather_rows(latent):
    half = latent.shape[1] // 2
    low2, high2 = shift(latent, "tp", 2), shift(latent, "tp", -2)
    low1, high1 = shift(latent, "tp", 1), shift(latent, "tp", -1)
    far = (shift(low2[:, :half], "tp", 2), shift(high2[:, half:], "tp", -2))
    low3, high3 = shift(low2, "tp", 1), shift(high2, "tp", -1)
    return [(low3,), (low2,), (low1,), (latent,), (high1,), (high2,), (high3,), far]


def reduce_rows(block):
    half = block(0).shape[1] // 2
    far = block(4)
    up4, down4 = shift(far[:, :half], "tp", 2), shift(far[:, half:], "tp", -2)
    up3, down3 = shift(block(3), "tp", 1), shift(block(-3), "tp", -1)
    up1, down1 = shift(block(1), "tp", 1), shift(block(-1), "tp", -1)
    gap = jnp.zeros_like(up4)
    two = added(block(2), up3, jnp.concatenate([up4, gap], axis=1))
    minus_two = added(block(-2), down3, jnp.concatenate([gap, down4], axis=1))
    up2, down2 = shift(two, "tp", 2), shift(minus_two, "tp", -2)
    total = block(0).astype(jnp.float32)
    for part in (up1, down1, up2, down2):
        total = total + part.astype(jnp.float32)
    return total


def angle_tables(positions):
    quarter = HEAD_SIZE // 4
    lane = jnp.arange(LANES, dtype=jnp.int32)
    entry = lane % (2 * quarter)
    exponent = (entry % quarter).astype(jnp.float32)
    inverse = jnp.exp(-math.log(10000.0) * exponent / quarter)
    grid_row = (positions // GRID_W).astype(jnp.float32)[:, None]
    grid_column = (positions % GRID_W).astype(jnp.float32)[:, None]
    angles = jnp.where(entry < quarter, grid_row, grid_column) * inverse
    sign = jnp.where(lane % HEAD_SIZE < HEAD_SIZE // 2, -1.0, 1.0)
    return jnp.cos(angles), jnp.sin(angles) * sign


def body(
    latent,
    condition,
    ctx_condition,
    context,
    mod_shift,
    mod_scale,
    mod_gate,
    norm_gain,
    w_query,
    key_weight,
    value_weight,
    w_gate,
    w_out,
    sink_logit,
):
    f32, bf16 = jnp.float32, jnp.bfloat16
    shape = jax.ShapeDtypeStruct
    sp_count, sp_rank = lax.axis_size("sp"), lax.axis_index("sp")
    tp_count, tp_rank = lax.axis_size("tp"), lax.axis_index("tp")
    own, width = latent.shape
    rows = own * tp_count
    mod_rows, columns = mod_shift.shape
    behind = (tp_count - 1) // 2

    conditions = jnp.stack(
        [
            lax.dynamic_slice_in_dim(vector, sp_rank * mod_rows, mod_rows, 0)
            for vector in (condition, ctx_condition)
        ]
    )
    acts = rounded(jax.nn.silu(conditions))
    parts = call(
        partial_kernel, shape((sp_count, 5, columns), f32), acts, mod_shift, mod_scale, mod_gate
    )
    pieces = gather_rows(latent)
    parts = copy_for_each(parts, "sp")
    totals = call(total_kernel, shape((tp_count, 5, columns), f32), parts)
    vectors = copy_for_each(totals, "tp")

    gain = norm_gain[None, :]
    kv_weight = jnp.concatenate([key_weight.T, value_weight.T], axis=0)
    offsets = (
        (tp_rank + tp_count - behind + jnp.arange(tp_count, dtype=jnp.int32)) % tp_count * own
    )
    begin = sp_rank * rows
    positions = begin + (offsets[:, None] + jnp.arange(own, dtype=jnp.int32)).reshape(rows)
    cosine, sine = angle_tables(positions)
    place = jnp.concatenate([jnp.stack([begin, rows * sp_count]).astype(jnp.int32), offsets])

    ctx_rows = context.shape[0]
    ctx_pair = call(
        context_kernel,
        shape((sp_count, ctx_rows, LANES), bf16),
        context,
        vectors,
        gain,
        kv_weight,
        scratch=[pltpu.VMEM((ctx_rows, width), bf16)],
    )
    ctx_all = copy_for_each(ctx_pair, "sp").reshape(sp_count * ctx_rows, LANES)

    blocks = [block for piece in pieces for block in piece]
    hidden, key_value, first, last = call(
        functools.partial(key_kernel, pieces=[[0] * len(p) for p in pieces], per_group=2),
        [
            shape((rows, width), bf16),
            shape((rows, LANES), bf16),
            shape((WINDOW, LANES), bf16),
            shape((WINDOW, LANES), bf16),
        ],
        place,
        *blocks,
        vectors,
        gain,
        kv_weight,
        cosine,
        sine,
        specs=[SMEM] + [VMEM] * (len(blocks) + 5),
        scratch=[pltpu.VMEM((rows, LANES), f32)],
    )
    low = shift(last, "sp", 1, wrap=False)
    high = shift(first, "sp", -1, wrap=False)
    heads = w_query.shape[1] // HEAD_SIZE
    queries, gate = call(
        functools.partial(query_kernel, own=own),
        [shape((rows * heads, LANES), f32), shape((rows, w_gate.shape[1]), f32)],
        hidden,
        w_query,
        w_gate,
        cosine,
        sine,
        specs=[VMEM, VMEM, ANY, VMEM, VMEM],
        scratch=[pltpu.VMEM(w_gate.shape, bf16), pltpu.SemaphoreType.DMA],
        flops=2 * 10**9,
    )
    span = 3 * LANES
    product = call(
        functools.partial(attend_kernel, own=own, span=span),
        shape((rows, width), bf16),
        place,
        sink_logit,
        queries,
        gate,
        low,
        key_value,
        high,
        ctx_all,
        w_out,
        specs=[SMEM, SMEM] + [VMEM] * 6 + [ANY],
        scratch=[
            pltpu.VMEM((rows - own + span, LANES), f32),
            pltpu.VMEM((rows, w_out.shape[0]), f32),
            pltpu.VMEM(w_out.shape, bf16),
            pltpu.SemaphoreType.DMA,
        ],
        flops=3 * 10**9,
    )
    branch = reduce_rows(lambda d: product[(d + behind) * own : (d + behind + 1) * own])
    lat_gate = vectors[:, 4, :].reshape(width)
    return rounded(latent.astype(f32) + lat_gate * branch)


def solution(mesh):
    return jax.shard_map(
        body,
        mesh=mesh,
        in_specs=(
            P(("dp", "sp", "tp"), None),
            P("dp"),
            P(),
            P(("dp", "sp"), None),
            P("sp", "tp"),
            P("sp", "tp"),
            P("sp", "tp"),
            P(),
            P(None, "tp"),
            P(None, "tp"),
            P(None, "tp"),
            P(None, "tp"),
            P("tp", None),
            P("tp"),
        ),
        out_specs=P(("dp", "sp", "tp"), None),
        check_vma=False,
    )
```

time: 161 us -> 135 us (0.84)
  the two profiles are of different devices: /device:TPU:6 before, /device:TPU:116 now
where the time goes in v3:
time: 135 us; the launch traced here: 134 us
  starting transfers between devices  92.9 us (69%)
  Pallas kernels  15.5 us (11%)
  waiting for transfers between devices  13.3 us (10%)
  local copies, waits for them, and re-layouts  9.14 us (7%)
  other arithmetic  2.47 us (2%)
    ppermute x18, starting transfers between devices, shift(): return lax.ppermute(block, axis, pairs)  60.3 us
    all_to_all x3, starting transfers between devices, copy_for_each(): return lax.all_to_all(copies, axis, split_axis=0, concat_axis=0, tiled=True)  32.6 us
    pallas_call x6, Pallas kernels, call(): pl.pallas_call(kernel, out_shape=out_shape, in_specs=specs or [VMEM] * le...  15.5 us
    ppermute x18, waiting for transfers between devices, shift(): return lax.ppermute(block, axis, pairs)  12.8 us
    unnamed x24, local copies, waits for them, and re-layouts  6.13 us
  transfers between devices with their start and end apart: 21, of which 4 were waited for; matrix products, arithmetic and copies ran while one was open for 3% of the time, Pallas kernels for 6%

profile of v3, /device:TPU:116, one launch (start us, length us, event | category | flops | bytes accessed | tf_op | source)
XLA Modules:
  0.0 133.7 jit_solution(2211662553594774986)
XLA Ops:
  1.9 4.8 %collective-permute-start.4 = (bf16[40,3072]{1,0:T(8,128)(2,1)}, bf16[40,3072]{1,0:T(8,128)(2,1)S(1)}, u32[]{:S(2)}, u32[]{:S(2)}) collective-permute-start(bf16[40,3072]{1,0:T(8,128)(2,1)} %refs_4_.1), channel_id=1, source_target_pairs={{0,48},{8,56},{16,0},{24,8},{32,16},{40,24},{48,32},{56,40},{1,49}... | collective-permute-start | bytes 737288 | tf_op jit(solution)/shard_map/ppermute | solution.py:253
  6.8 2.6 %collective-permute-start.2 = (bf16[40,3072]{1,0:T(8,128)(2,1)}, bf16[40,3072]{1,0:T(8,128)(2,1)S(1)}, u32[]{:S(2)}, u32[]{:S(2)}) collective-permute-start(bf16[40,3072]{1,0:T(8,128)(2,1)} %refs_4_.1), channel_id=1, source_target_pairs={{0,8},{8,16},{16,24},{24,32},{32,40},{40,48},{48,56},{56,0},{1,9},... | collective-permute-start | bytes 737288 | tf_op jit(solution)/shard_map/ppermute | solution.py:253
  9.3 3.8 %collective-permute-start.3 = (bf16[40,3072]{1,0:T(8,128)(2,1)}, bf16[40,3072]{1,0:T(8,128)(2,1)S(1)}, u32[]{:S(2)}, u32[]{:S(2)}) collective-permute-start(bf16[40,3072]{1,0:T(8,128)(2,1)} %refs_4_.1), channel_id=1, source_target_pairs={{0,56},{8,0},{16,8},{24,16},{32,24},{40,32},{48,40},{56,48},{1,57}... | collective-permute-start | bytes 737288 | tf_op jit(solution)/shard_map/ppermute | solution.py:253
  18.4 14.8 %all-to-all-start = ((f32[12,5,384]{2,1,0:T(8,128)}), f32[12,5,384]{2,1,0:T(8,128)S(1)}, u32[]{:S(2)}, u32[]{:S(2)}) async-start(f32[12,5,384]{2,1,0:T(8,128)} %shard_map.136), calls=%async_computation | async-start | bytes 294912 | tf_op jit(solution)/shard_map/all_to_all | solution.py:247
  35.3 3.8 %collective-permute-start.6 = (bf16[40,1536]{1,0:T(8,128)(2,1)}, bf16[40,1536]{1,0:T(8,128)(2,1)S(1)}, u32[]{:S(2)}, u32[]{:S(2)}) collective-permute-start(bf16[40,1536]{1,0:T(8,128)(2,1)} %slice.52), channel_id=1, source_target_pairs={{0,16},{8,24},{16,32},{24,40},{32,48},{40,56},{48,0},{56,8},{1,17}... | collective-permute-start | bytes 368648 | tf_op jit(solution)/shard_map/ppermute | solution.py:253
  39.1 2.1 %collective-permute-start.1 = (bf16[40,3072]{1,0:T(8,128)(2,1)S(1)}, bf16[40,3072]{1,0:T(8,128)(2,1)S(1)}, u32[]{:S(2)}, u32[]{:S(2)}) collective-permute-start(bf16[40,3072]{1,0:T(8,128)(2,1)S(1)} %collective-permute-done.refs_2_), channel_id=1, source_target_pairs={{0,8},{8,16},{16,24},{24,32},{32,40},{40,48},{48,56},{56,0},{1,9},... | collective-permute-start | bytes 737288 | tf_op jit(solution)/shard_map/ppermute | solution.py:253
  41.2 3.7 %collective-permute-start.5 = (bf16[40,3072]{1,0:T(8,128)(2,1)S(1)}, bf16[40,3072]{1,0:T(8,128)(2,1)S(1)}, u32[]{:S(2)}, u32[]{:S(2)}) collective-permute-start(bf16[40,3072]{1,0:T(8,128)(2,1)S(1)} %collective-permute-done.4.refs_6_), channel_id=1, source_target_pairs={{0,56},{8,0},{16,8},{24,16},{32,24},{40,32},{48,40},{56,48},{1,57}... | collective-permute-start | bytes 737288 | tf_op jit(solution)/shard_map/ppermute | solution.py:253
  46.2 8.2 %all-to-all-start.1 = ((f32[8,5,384]{2,1,0:T(8,128)}), f32[8,5,384]{2,1,0:T(8,128)S(1)}, u32[]{:S(2)}, u32[]{:S(2)}) async-start(f32[8,5,384]{2,1,0:T(8,128)} %shard_map.137), calls=%async_computation.1 | async-start | bytes 196608 | tf_op jit(solution)/shard_map/all_to_all | solution.py:247
  54.4 4.4 %collective-permute-start.7 = (bf16[40,1536]{1,0:T(8,128)(2,1)}, bf16[40,1536]{1,0:T(8,128)(2,1)S(1)}, u32[]{:S(2)}, u32[]{:S(2)}) collective-permute-start(bf16[40,1536]{1,0:T(8,128)(2,1)} %slice.53), channel_id=1, source_target_pairs={{0,48},{8,56},{16,0},{24,8},{32,16},{40,24},{48,32},{56,40},{1,49}... | collective-permute-start | bytes 368648 | tf_op jit(solution)/shard_map/ppermute | solution.py:253
  60.6 9.6 %all-to-all-start.2 = ((bf16[12,32,128]{2,1,0:T(8,128)(2,1)}), bf16[12,32,128]{2,1,0:T(8,128)(2,1)S(1)}, u32[]{:S(2)}, u32[]{:S(2)}) async-start(bf16[12,32,128]{2,1,0:T(8,128)(2,1)} %shard_map.140), calls=%async_computation.2 | async-start | bytes 196608 | tf_op jit(solution)/shard_map/all_to_all | solution.py:247
  70.2 2.1 %shard_map.138 = (bf16[320,3072]{1,0:T(8,128)(2,1)S(1)}, bf16[320,128]{1,0:T(8,128)(2,1)S(1)}, bf16[128,128]{1,0:T(8,128)(2,1)S(1)}, bf16[128,128]{1,0:T(8,128)(2,1)S(1)}) custom-call(s32[10]{0:T(128)S(1)} %pad_add_fusion.refs_0_.place, bf16[40,3072]{1,0:T(8,128)(2,1)S(1)} %collective-permute-done.1.refs_1_, ...), custom_call_target="tpu_custom_call" | custom-call | flops 1000000000 | bytes 1000000 | tf_op jit(solution)/shard_map/pallas_call | solution.py:33
  72.3 3.4 %collective-permute-start.8 = (bf16[128,128]{1,0:T(8,128)(2,1)S(1)}, bf16[128,128]{1,0:T(8,128)(2,1)S(1)}, u32[]{:S(2)}, u32[]{:S(2)}) collective-permute-start(bf16[128,128]{1,0:T(8,128)(2,1)S(1)} %get-tuple-element.14), channel_id=1, source_target_pairs={{0,64},{64,128},{128,192},{192,256},{256,320},{320,384},{384,448},... | collective-permute-start | bytes 98312 | tf_op jit(solution)/shard_map/ppermute | solution.py:253
  75.7 2.6 %collective-permute-start.9 = (bf16[128,128]{1,0:T(8,128)(2,1)S(1)}, bf16[128,128]{1,0:T(8,128)(2,1)S(1)}, u32[]{:S(2)}, u32[]{:S(2)}) collective-permute-start(bf16[128,128]{1,0:T(8,128)(2,1)S(1)} %get-tuple-element.16), channel_id=1, source_target_pairs={{64,0},{128,64},{192,128},{256,192},{320,256},{384,320},{448,384},... | collective-permute-start | bytes 98312 | tf_op jit(solution)/shard_map/ppermute | solution.py:253
  80.0 2.9 %shard_map.139 = (f32[1920,128]{1,0:T(8,128)S(1)}, f32[320,384]{1,0:T(8,128)S(1)}) custom-call(bf16[320,3072]{1,0:T(8,128)(2,1)S(1)} %get-tuple-element.11.hidden, bf16[3072,384]{1,0:T(8,128)(2,1)S(1)} %copy-done.1, bf16[3072,384]{1,0:T(8,128)(2,1)S(1)} %copy-done.2, f32[320,128]{1,0:T(8,128)S(1)} %get-tuple-element.26.refs_13_.cosine, ...), custom_call_target="tpu_custom_call" | custom-call | flops 2000000000 | bytes 1000000 | tf_op jit(solution)/shard_map/pallas_call | solution.py:33
  84.6 7.9 %shard_map.141 = bf16[320,3072]{1,0:T(8,128)(2,1)S(1)} custom-call(s32[10]{0:T(128)S(1)} %pad_add_fusion.refs_0_.place, f32[6]{0:T(128)S(1)} %copy-done.9, f32[1920,128]{1,0:T(8,128)S(1)} %get-tuple-element.12.queries, f32[320,384]{1,0:T(8,128)S(1)} %get-tuple-element.13.gate, bf16[128,128]{1,0:T(8,128)(2,1)S(1)} %collective-permute-done.8.low, ...), custom_call_target="tpu_custom_call" | custom-call | flops 3000000000 | bytes 1000000 | tf_op jit(solution)/shard_map/pallas_call | solution.py:33
  92.6 4.5 %collective-permute-start.12 = (bf16[40,3072]{1,0:T(8,128)(2,1)S(1)}, bf16[40,3072]{1,0:T(8,128)(2,1)S(1)}, u32[]{:S(2)}, u32[]{:S(2)}) collective-permute-start(bf16[40,3072]{1,0:T(8,128)(2,1)S(1)} %get-tuple-element.19), channel_id=1, source_target_pairs={{0,8},{8,16},{16,24},{24,32},{32,40},{40,48},{48,56},{56,0},{1,9},... | collective-permute-start | bytes 737288 | tf_op jit(solution)/shard_map/ppermute | solution.py:253
  99.1 6.2 %collective-permute-start.13 = (bf16[40,1536]{1,0:T(8,128)(2,1)S(1)}, bf16[40,1536]{1,0:T(8,128)(2,1)S(1)}, u32[]{:S(2)}, u32[]{:S(2)}) collective-permute-start(bf16[40,1536]{1,0:T(8,128)(2,1)S(1)} %get-tuple-element.23), channel_id=1, source_target_pairs={{0,16},{8,24},{16,32},{24,40},{32,48},{40,56},{48,0},{56,8},{1,17}... | collective-permute-start | bytes 368648 | tf_op jit(solution)/shard_map/ppermute | solution.py:253
  107.3 2.6 %collective-permute-start.10 = (bf16[40,3072]{1,0:T(8,128)(2,1)S(1)}, bf16[40,3072]{1,0:T(8,128)(2,1)S(1)}, u32[]{:S(2)}, u32[]{:S(2)}) collective-permute-start(bf16[40,3072]{1,0:T(8,128)(2,1)S(1)} %get-tuple-element.17), channel_id=1, source_target_pairs={{0,8},{8,16},{16,24},{24,32},{32,40},{40,48},{48,56},{56,0},{1,9},... | collective-permute-start | bytes 737288 | tf_op jit(solution)/shard_map/ppermute | solution.py:253
  109.8 3.3 %collective-permute-start.11 = (bf16[40,3072]{1,0:T(8,128)(2,1)S(1)}, bf16[40,3072]{1,0:T(8,128)(2,1)S(1)}, u32[]{:S(2)}, u32[]{:S(2)}) collective-permute-start(bf16[40,3072]{1,0:T(8,128)(2,1)S(1)} %get-tuple-element.20), channel_id=1, source_target_pairs={{0,56},{8,0},{16,8},{24,16},{32,24},{40,32},{48,40},{56,48},{1,57}... | collective-permute-start | bytes 737288 | tf_op jit(solution)/shard_map/ppermute | solution.py:253
  113.1 3.7 %collective-permute-done.16 = bf16[40,1536]{1,0:T(8,128)(2,1)S(1)} collective-permute-done((bf16[40,1536]{1,0:T(8,128)(2,1)S(1)}, bf16[40,1536]{1,0:T(8,128)(2,1)S(1)}, u32[]{:S(2)}, u32[]{:S(2)}) %collective-permute-start.16) | collective-permute-done | bytes 122912 | tf_op jit(solution)/shard_map/ppermute | solution.py:253
  117.0 3.5 %collective-permute-start.14 = (bf16[40,3072]{1,0:T(8,128)(2,1)S(1)}, bf16[40,3072]{1,0:T(8,128)(2,1)S(1)}, u32[]{:S(2)}, u32[]{:S(2)}) collective-permute-start(bf16[40,3072]{1,0:T(8,128)(2,1)S(1)} %get-tuple-element.21), channel_id=1, source_target_pairs={{0,16},{8,24},{16,32},{24,40},{32,48},{40,56},{48,0},{56,8},{1,17}... | collective-permute-start | bytes 737288 | tf_op jit(solution)/shard_map/ppermute | solution.py:253
  120.6 3.2 %collective-permute-start.17 = (bf16[40,3072]{1,0:T(8,128)(2,1)S(1)}, bf16[40,3072]{1,0:T(8,128)(2,1)S(1)}, u32[]{:S(2)}, u32[]{:S(2)}) collective-permute-start(bf16[40,3072]{1,0:T(8,128)(2,1)S(1)} %get-tuple-element.22), channel_id=1, source_target_pairs={{0,48},{8,56},{16,0},{24,8},{32,16},{40,24},{48,32},{56,40},{1,49}... | collective-permute-start | bytes 737288 | tf_op jit(solution)/shard_map/ppermute | solution.py:253
  123.8 3.6 %collective-permute-done.14 = bf16[40,3072]{1,0:T(8,128)(2,1)S(1)} collective-permute-done((bf16[40,3072]{1,0:T(8,128)(2,1)S(1)}, bf16[40,3072]{1,0:T(8,128)(2,1)S(1)}, u32[]{:S(2)}, u32[]{:S(2)}) %collective-permute-start.14) | collective-permute-done | bytes 245792 | tf_op jit(solution)/shard_map/ppermute | solution.py:253
  127.4 5.4 %collective-permute-done.17 = bf16[40,3072]{1,0:T(8,128)(2,1)S(1)} collective-permute-done((bf16[40,3072]{1,0:T(8,128)(2,1)S(1)}, bf16[40,3072]{1,0:T(8,128)(2,1)S(1)}, u32[]{:S(2)}, u32[]{:S(2)}) %collective-permute-start.17) | collective-permute-done | bytes 245792 | tf_op jit(solution)/shard_map/ppermute | solution.py:253
  (67 shorter events, 20.5 us)
Async XLA Ops:
  0.0 34.6 %collective-permute-start = (bf16[40,3072]{1,0:T(8,128)(2,1)}, bf16[40,3072]{1,0:T(8,128)(2,1)S(1)}, u32[]{:S(2)}, u32[]{:S(2)}) collective-permute-start(bf16[40,3072]{1,0:T(8,128)(2,1)} %refs_4_.1), channel_id=1, source_target_pairs={{0,16},{8,24},{16,32},{24,40},{32,48},{40,56},{48,0},{56,8},{1,17}... | collective-permute-start | bytes 737288 | tf_op jit(solution)/shard_map/ppermute | solution.py:253
  1.9 39.3 %collective-permute-start.4 = (bf16[40,3072]{1,0:T(8,128)(2,1)}, bf16[40,3072]{1,0:T(8,128)(2,1)S(1)}, u32[]{:S(2)}, u32[]{:S(2)}) collective-permute-start(bf16[40,3072]{1,0:T(8,128)(2,1)} %refs_4_.1), channel_id=1, source_target_pairs={{0,48},{8,56},{16,0},{24,8},{32,16},{40,24},{48,32},{56,40},{1,49}... | collective-permute-start | bytes 737288 | tf_op jit(solution)/shard_map/ppermute | solution.py:253
  6.8 47.7 %collective-permute-start.2 = (bf16[40,3072]{1,0:T(8,128)(2,1)}, bf16[40,3072]{1,0:T(8,128)(2,1)S(1)}, u32[]{:S(2)}, u32[]{:S(2)}) collective-permute-start(bf16[40,3072]{1,0:T(8,128)(2,1)} %refs_4_.1), channel_id=1, source_target_pairs={{0,8},{8,16},{16,24},{24,32},{32,40},{40,48},{48,56},{56,0},{1,9},... | collective-permute-start | bytes 737288 | tf_op jit(solution)/shard_map/ppermute | solution.py:253
  9.3 60.8 %collective-permute-start.3 = (bf16[40,3072]{1,0:T(8,128)(2,1)}, bf16[40,3072]{1,0:T(8,128)(2,1)S(1)}, u32[]{:S(2)}, u32[]{:S(2)}) collective-permute-start(bf16[40,3072]{1,0:T(8,128)(2,1)} %refs_4_.1), channel_id=1, source_target_pairs={{0,56},{8,0},{16,8},{24,16},{32,24},{40,32},{48,40},{56,48},{1,57}... | collective-permute-start | bytes 737288 | tf_op jit(solution)/shard_map/ppermute | solution.py:253
  17.5 15.9 %copy-start.10 = (bf16[3072,64]{0,1:T(8,128)(2,1)S(1)}, bf16[3072,64]{0,1:T(8,128)(2,1)}, u32[]{:S(2)}) copy-start(bf16[3072,64]{0,1:T(8,128)(2,1)} %param.24) | copy-start | bytes 1179652
  17.5 15.9 %copy-start.11 = (bf16[3072,64]{0,1:T(8,128)(2,1)S(1)}, bf16[3072,64]{0,1:T(8,128)(2,1)}, u32[]{:S(2)}) copy-start(bf16[3072,64]{0,1:T(8,128)(2,1)} %param.23) | copy-start | bytes 1179652
  18.4 27.2 %all-to-all-start = ((f32[12,5,384]{2,1,0:T(8,128)}), f32[12,5,384]{2,1,0:T(8,128)S(1)}, u32[]{:S(2)}, u32[]{:S(2)}) async-start(f32[12,5,384]{2,1,0:T(8,128)} %shard_map.136), calls=%async_computation | async-start | bytes 294912 | tf_op jit(solution)/shard_map/all_to_all | solution.py:247
  35.3 34.9 %collective-permute-start.6 = (bf16[40,1536]{1,0:T(8,128)(2,1)}, bf16[40,1536]{1,0:T(8,128)(2,1)S(1)}, u32[]{:S(2)}, u32[]{:S(2)}) collective-permute-start(bf16[40,1536]{1,0:T(8,128)(2,1)} %slice.52), channel_id=1, source_target_pairs={{0,16},{8,24},{16,32},{24,40},{32,48},{40,56},{48,0},{56,8},{1,17}... | collective-permute-start | bytes 368648 | tf_op jit(solution)/shard_map/ppermute | solution.py:253
  39.1 31.1 %collective-permute-start.1 = (bf16[40,3072]{1,0:T(8,128)(2,1)S(1)}, bf16[40,3072]{1,0:T(8,128)(2,1)S(1)}, u32[]{:S(2)}, u32[]{:S(2)}) collective-permute-start(bf16[40,3072]{1,0:T(8,128)(2,1)S(1)} %collective-permute-done.refs_2_), channel_id=1, source_target_pairs={{0,8},{8,16},{16,24},{24,32},{32,40},{40,48},{48,56},{56,0},{1,9},... | collective-permute-start | bytes 737288 | tf_op jit(solution)/shard_map/ppermute | solution.py:253
  41.2 29.0 %collective-permute-start.5 = (bf16[40,3072]{1,0:T(8,128)(2,1)S(1)}, bf16[40,3072]{1,0:T(8,128)(2,1)S(1)}, u32[]{:S(2)}, u32[]{:S(2)}) collective-permute-start(bf16[40,3072]{1,0:T(8,128)(2,1)S(1)} %collective-permute-done.4.refs_6_), channel_id=1, source_target_pairs={{0,56},{8,0},{16,8},{24,16},{32,24},{40,32},{48,40},{56,48},{1,57}... | collective-permute-start | bytes 737288 | tf_op jit(solution)/shard_map/ppermute | solution.py:253
  46.2 13.2 %all-to-all-start.1 = ((f32[8,5,384]{2,1,0:T(8,128)}), f32[8,5,384]{2,1,0:T(8,128)S(1)}, u32[]{:S(2)}, u32[]{:S(2)}) async-start(f32[8,5,384]{2,1,0:T(8,128)} %shard_map.137), calls=%async_computation.1 | async-start | bytes 196608 | tf_op jit(solution)/shard_map/all_to_all | solution.py:247
  54.4 15.8 %copy-start = (bf16[40,3072]{1,0:T(8,128)(2,1)S(1)}, bf16[40,3072]{1,0:T(8,128)(2,1)}, u32[]{:S(2)}) copy-start(bf16[40,3072]{1,0:T(8,128)(2,1)} %refs_4_.1) | copy-start | bytes 737284
  54.4 15.7 %collective-permute-start.7 = (bf16[40,1536]{1,0:T(8,128)(2,1)}, bf16[40,1536]{1,0:T(8,128)(2,1)S(1)}, u32[]{:S(2)}, u32[]{:S(2)}) collective-permute-start(bf16[40,1536]{1,0:T(8,128)(2,1)} %slice.53), channel_id=1, source_target_pairs={{0,48},{8,56},{16,0},{24,8},{32,16},{40,24},{48,32},{56,40},{1,49}... | collective-permute-start | bytes 368648 | tf_op jit(solution)/shard_map/ppermute | solution.py:253
  60.6 22.4 %all-to-all-start.2 = ((bf16[12,32,128]{2,1,0:T(8,128)(2,1)}), bf16[12,32,128]{2,1,0:T(8,128)(2,1)S(1)}, u32[]{:S(2)}, u32[]{:S(2)}) async-start(bf16[12,32,128]{2,1,0:T(8,128)(2,1)} %shard_map.140), calls=%async_computation.2 | async-start | bytes 196608 | tf_op jit(solution)/shard_map/all_to_all | solution.py:247
  72.3 10.6 %collective-permute-start.8 = (bf16[128,128]{1,0:T(8,128)(2,1)S(1)}, bf16[128,128]{1,0:T(8,128)(2,1)S(1)}, u32[]{:S(2)}, u32[]{:S(2)}) collective-permute-start(bf16[128,128]{1,0:T(8,128)(2,1)S(1)} %get-tuple-element.14), channel_id=1, source_target_pairs={{0,64},{64,128},{128,192},{192,256},{256,320},{320,384},{384,448},... | collective-permute-start | bytes 98312 | tf_op jit(solution)/shard_map/ppermute | solution.py:253
  75.7 7.2 %collective-permute-start.9 = (bf16[128,128]{1,0:T(8,128)(2,1)S(1)}, bf16[128,128]{1,0:T(8,128)(2,1)S(1)}, u32[]{:S(2)}, u32[]{:S(2)}) collective-permute-start(bf16[128,128]{1,0:T(8,128)(2,1)S(1)} %get-tuple-element.16), channel_id=1, source_target_pairs={{64,0},{128,64},{192,128},{256,192},{320,256},{384,320},{448,384},... | collective-permute-start | bytes 98312 | tf_op jit(solution)/shard_map/ppermute | solution.py:253
  92.6 24.2 %collective-permute-start.12 = (bf16[40,3072]{1,0:T(8,128)(2,1)S(1)}, bf16[40,3072]{1,0:T(8,128)(2,1)S(1)}, u32[]{:S(2)}, u32[]{:S(2)}) collective-permute-start(bf16[40,3072]{1,0:T(8,128)(2,1)S(1)} %get-tuple-element.19), channel_id=1, source_target_pairs={{0,8},{8,16},{16,24},{24,32},{32,40},{40,48},{48,56},{56,0},{1,9},... | collective-permute-start | bytes 737288 | tf_op jit(solution)/shard_map/ppermute | solution.py:253
  97.1 19.7 %collective-permute-start.15 = (bf16[40,3072]{1,0:T(8,128)(2,1)S(1)}, bf16[40,3072]{1,0:T(8,128)(2,1)S(1)}, u32[]{:S(2)}, u32[]{:S(2)}) collective-permute-start(bf16[40,3072]{1,0:T(8,128)(2,1)S(1)} %get-tuple-element.18), channel_id=1, source_target_pairs={{0,56},{8,0},{16,8},{24,16},{32,24},{40,32},{48,40},{56,48},{1,57}... | collective-permute-start | bytes 737288 | tf_op jit(solution)/shard_map/ppermute | solution.py:253
  99.1 10.7 %collective-permute-start.13 = (bf16[40,1536]{1,0:T(8,128)(2,1)S(1)}, bf16[40,1536]{1,0:T(8,128)(2,1)S(1)}, u32[]{:S(2)}, u32[]{:S(2)}) collective-permute-start(bf16[40,1536]{1,0:T(8,128)(2,1)S(1)} %get-tuple-element.23), channel_id=1, source_target_pairs={{0,16},{8,24},{16,32},{24,40},{32,48},{40,56},{48,0},{56,8},{1,17}... | collective-permute-start | bytes 368648 | tf_op jit(solution)/shard_map/ppermute | solution.py:253
  105.3 11.5 %collective-permute-start.16 = (bf16[40,1536]{1,0:T(8,128)(2,1)S(1)}, bf16[40,1536]{1,0:T(8,128)(2,1)S(1)}, u32[]{:S(2)}, u32[]{:S(2)}) collective-permute-start(bf16[40,1536]{1,0:T(8,128)(2,1)S(1)} %get-tuple-element.24), channel_id=1, source_target_pairs={{0,48},{8,56},{16,0},{24,8},{32,16},{40,24},{48,32},{56,40},{1,49}... | collective-permute-start | bytes 368648 | tf_op jit(solution)/shard_map/ppermute | solution.py:253
  107.3 16.5 %collective-permute-start.10 = (bf16[40,3072]{1,0:T(8,128)(2,1)S(1)}, bf16[40,3072]{1,0:T(8,128)(2,1)S(1)}, u32[]{:S(2)}, u32[]{:S(2)}) collective-permute-start(bf16[40,3072]{1,0:T(8,128)(2,1)S(1)} %get-tuple-element.17), channel_id=1, source_target_pairs={{0,8},{8,16},{16,24},{24,32},{32,40},{40,48},{48,56},{56,0},{1,9},... | collective-permute-start | bytes 737288 | tf_op jit(solution)/shard_map/ppermute | solution.py:253
  109.8 14.0 %collective-permute-start.11 = (bf16[40,3072]{1,0:T(8,128)(2,1)S(1)}, bf16[40,3072]{1,0:T(8,128)(2,1)S(1)}, u32[]{:S(2)}, u32[]{:S(2)}) collective-permute-start(bf16[40,3072]{1,0:T(8,128)(2,1)S(1)} %get-tuple-element.20), channel_id=1, source_target_pairs={{0,56},{8,0},{16,8},{24,16},{32,24},{40,32},{48,40},{56,48},{1,57}... | collective-permute-start | bytes 737288 | tf_op jit(solution)/shard_map/ppermute | solution.py:253
  117.0 10.4 %collective-permute-start.14 = (bf16[40,3072]{1,0:T(8,128)(2,1)S(1)}, bf16[40,3072]{1,0:T(8,128)(2,1)S(1)}, u32[]{:S(2)}, u32[]{:S(2)}) collective-permute-start(bf16[40,3072]{1,0:T(8,128)(2,1)S(1)} %get-tuple-element.21), channel_id=1, source_target_pairs={{0,16},{8,24},{16,32},{24,40},{32,48},{40,56},{48,0},{56,8},{1,17}... | collective-permute-start | bytes 737288 | tf_op jit(solution)/shard_map/ppermute | solution.py:253
  120.6 12.3 %collective-permute-start.17 = (bf16[40,3072]{1,0:T(8,128)(2,1)S(1)}, bf16[40,3072]{1,0:T(8,128)(2,1)S(1)}, u32[]{:S(2)}, u32[]{:S(2)}) collective-permute-start(bf16[40,3072]{1,0:T(8,128)(2,1)S(1)} %get-tuple-element.22), channel_id=1, source_target_pairs={{0,48},{8,56},{16,0},{24,8},{32,16},{40,24},{48,32},{56,40},{1,49}... | collective-permute-start | bytes 737288 | tf_op jit(solution)/shard_map/ppermute | solution.py:253
  (9 other events, 45.0 us)

commit v4 on v3

--- a/solution.py
+++ b/solution.py
@@ -15,7 +15,7 @@
 NORM_EPS = 1e-06
 MASK_VALUE = -1e30
 VMEM = pl.BlockSpec(memory_space=pltpu.VMEM)
-ANY = pl.BlockSpec(memory_space=pl.ANY)
+HBM = pl.BlockSpec(memory_space=pltpu.HBM)
 SMEM = pl.BlockSpec(memory_space=pltpu.SMEM)
 
 
@@ -29,30 +29,31 @@
     )
 
 
-def call(kernel, out_shape, *operands, specs=None, scratch=(), flops=10**9):
+def call(kernel, out_shape, *operands, specs=None, scratch=(), flops=10**9, grant=30):
     return pl.pallas_call(
         kernel,
         out_shape=out_shape,
         in_specs=specs or [VMEM] * len(operands),
         out_specs=jax.tree.map(lambda _: VMEM, out_shape),
         scratch_shapes=scratch,
-        compiler_params=pltpu.CompilerParams(vmem_limit_bytes=VMEM_GRANT),
+        compiler_params=pltpu.CompilerParams(vmem_limit_bytes=grant * 2**20),
         cost_estimate=pl.CostEstimate(flops=flops, bytes_accessed=10**6, transcendentals=0),
     )(*operands)
 
 
-VMEM_GRANT = 30 * 2**20
-
-
-def partial_kernel(acts, shift, scale, gate, out):
-    sums = jnp.concatenate(
-        [
-            contract(acts[...], shift[...]),
-            contract(acts[...], scale[...]),
-            contract(acts[...], gate[...])[:1],
-        ],
-        axis=0,
-    )
+def partial_kernel(rank, conditions, shift, scale, gate, out, held, ready):
+    fetches = []
+    for index, weight in enumerate((shift, scale, gate)):
+        fetches.append(pltpu.make_async_copy(weight, held.at[index], ready.at[index]))
+        fetches[-1].start()
+    mine = pl.ds(rank[0], 1)
+    values = jnp.concatenate([conditions[0, mine, :], conditions[1, mine, :]], axis=0)
+    acts = rounded(values / (1.0 + jnp.exp(-values)))
+    sums = []
+    for index, fetch in enumerate(fetches):
+        fetch.wait()
+        sums.append(contract(acts, held[index]))
+    sums = jnp.concatenate([sums[0], sums[1], sums[2][:1]], axis=0)
     for copy in range(out.shape[0]):
         out[copy] = sums
 
@@ -260,25 +261,32 @@
     return rounded(total)
 
 
-def gather_rows(latent):
-    half = latent.shape[1] // 2
+def shift_by_parity(block, steps):
+    tp_count, dp_count = lax.axis_size("tp"), lax.axis_size("dp")
+    pairs = []
+    for i in range(tp_count):
+        for j in range(dp_count):
+            target = (i + (steps if j % 2 == 0 else -steps)) % tp_count
+            pairs.append((i * dp_count + j, target * dp_count + j))
+    return lax.ppermute(block, ("tp", "dp"), pairs)
+
+
+def gather_rows(latent, even):
     low2, high2 = shift(latent, "tp", 2), shift(latent, "tp", -2)
     low1, high1 = shift(latent, "tp", 1), shift(latent, "tp", -1)
-    far = (shift(low2[:, :half], "tp", 2), shift(high2[:, half:], "tp", -2))
+    far = shift_by_parity(jnp.where(even, low2, high2), 2)
     low3, high3 = shift(low2, "tp", 1), shift(high2, "tp", -1)
-    return [(low3,), (low2,), (low1,), (latent,), (high1,), (high2,), (high3,), far]
-
-
-def reduce_rows(block):
-    half = block(0).shape[1] // 2
-    far = block(4)
-    up4, down4 = shift(far[:, :half], "tp", 2), shift(far[:, half:], "tp", -2)
+    return [(low3,), (low2,), (low1,), (latent,), (high1,), (high2,), (high3,), (far,)]
+
+
+def reduce_rows(block, even):
+    far = shift_by_parity(block(4), 2)
     up3, down3 = shift(block(3), "tp", 1), shift(block(-3), "tp", -1)
+    nothing = jnp.zeros_like(far)
+    two = added(block(2), up3, jnp.where(even, far, nothing))
+    minus_two = added(block(-2), down3, jnp.where(even, nothing, far))
+    up2, down2 = shift(two, "tp", 2), shift(minus_two, "tp", -2)
     up1, down1 = shift(block(1), "tp", 1), shift(block(-1), "tp", -1)
-    gap = jnp.zeros_like(up4)
-    two = added(block(2), up3, jnp.concatenate([up4, gap], axis=1))
-    minus_two = added(block(-2), down3, jnp.concatenate([gap, down4], axis=1))
-    up2, down2 = shift(two, "tp", 2), shift(minus_two, "tp", -2)
     total = block(0).astype(jnp.float32)
     for part in (up1, down1, up2, down2):
         total = total + part.astype(jnp.float32)
@@ -323,17 +331,21 @@
     mod_rows, columns = mod_shift.shape
     behind = (tp_count - 1) // 2
 
-    conditions = jnp.stack(
-        [
-            lax.dynamic_slice_in_dim(vector, sp_rank * mod_rows, mod_rows, 0)
-            for vector in (condition, ctx_condition)
-        ]
-    )
-    acts = rounded(jax.nn.silu(conditions))
+    conditions = jnp.stack([condition, ctx_condition]).reshape(2, sp_count, mod_rows)
     parts = call(
-        partial_kernel, shape((sp_count, 5, columns), f32), acts, mod_shift, mod_scale, mod_gate
-    )
-    pieces = gather_rows(latent)
+        partial_kernel,
+        shape((sp_count, 5, columns), f32),
+        sp_rank.astype(jnp.int32)[None],
+        conditions,
+        mod_shift,
+        mod_scale,
+        mod_gate,
+        specs=[SMEM, VMEM, HBM, HBM, HBM],
+        scratch=[pltpu.VMEM((3, mod_rows, columns), bf16), pltpu.SemaphoreType.DMA((3,))],
+        grant=63,
+    )
+    even = lax.axis_index("dp") % 2 == 0
+    pieces = gather_rows(latent, even)
     parts = copy_for_each(parts, "sp")
     totals = call(total_kernel, shape((tp_count, 5, columns), f32), parts)
     vectors = copy_for_each(totals, "tp")
@@ -390,9 +402,10 @@
         w_gate,
         cosine,
         sine,
-        specs=[VMEM, VMEM, ANY, VMEM, VMEM],
+        specs=[VMEM, VMEM, HBM, VMEM, VMEM],
         scratch=[pltpu.VMEM(w_gate.shape, bf16), pltpu.SemaphoreType.DMA],
         flops=2 * 10**9,
+        grant=48,
     )
     span = 3 * LANES
     product = call(
@@ -407,7 +420,7 @@
         high,
         ctx_all,
         w_out,
-        specs=[SMEM, SMEM] + [VMEM] * 6 + [ANY],
+        specs=[SMEM, SMEM] + [VMEM] * 6 + [HBM],
         scratch=[
             pltpu.VMEM((rows - own + span, LANES), f32),
             pltpu.VMEM((rows, w_out.shape[0]), f32),
@@ -415,8 +428,9 @@
             pltpu.SemaphoreType.DMA,
         ],
         flops=3 * 10**9,
-    )
-    branch = reduce_rows(lambda d: product[(d + behind) * own : (d + behind + 1) * own])
+        grant=50,
+    )
+    branch = reduce_rows(lambda d: product[(d + behind) * own : (d + behind + 1) * own], even)
     lat_gate = vectors[:, 4, :].reshape(width)
     return rounded(latent.astype(f32) + lat_gate * branch)
 

time: 135 us -> 129 us (0.956)
  the two profiles are of different devices: /device:TPU:116 before, /device:TPU:50 now
where the time goes in v4:
time: 129 us; the launch traced here: 128 us
  starting transfers between devices  86.1 us (67%)
  Pallas kernels  18 us (14%)
  waiting for transfers between devices  16.6 us (13%)
  other arithmetic  4.95 us (4%)
  local copies, waits for them, and re-layouts  2.27 us (2%)
    ppermute x14, starting transfers between devices, shift(): return lax.ppermute(block, axis, pairs)  44.1 us
    all_to_all x3, starting transfers between devices, copy_for_each(): return lax.all_to_all(copies, axis, split_axis=0, concat_axis=0, tiled=True)  33 us
    pallas_call x6, Pallas kernels, call(): pl.pallas_call(kernel, out_shape=out_shape, in_specs=specs or [VMEM] * le...  18 us
    ppermute x14, waiting for transfers between devices, shift(): return lax.ppermute(block, axis, pairs)  11.7 us
    ppermute x2, starting transfers between devices, shift_by_parity(): return lax.ppermute(block, ('tp', 'dp'), pairs)  9.02 us
    all_to_all x3, waiting for transfers between devices, copy_for_each(): return lax.all_to_all(copies, axis, split_axis=0, concat_axis=0, tiled=True)  4.92 us
  transfers between devices with their start and end apart: 19, of which 5 were waited for; matrix products, arithmetic and copies ran while one was open for 4% of the time, Pallas kernels for 7%

profile of v4, /device:TPU:50, one launch (start us, length us, event | category | flops | bytes accessed | tf_op | source)
XLA Modules:
  0.0 128.4 jit_solution(18284617292335034894)
XLA Ops:
  1.9 4.8 %collective-permute-start.4 = (bf16[40,3072]{1,0:T(8,128)(2,1)}, bf16[40,3072]{1,0:T(8,128)(2,1)S(1)}, u32[]{:S(2)}, u32[]{:S(2)}) collective-permute-start(bf16[40,3072]{1,0:T(8,128)(2,1)} %refs_4_.1), channel_id=1, source_target_pairs={{0,48},{8,56},{16,0},{24,8},{32,16},{40,24},{48,32},{56,40},{1,49}... | collective-permute-start | bytes 737288 | tf_op jit(solution)/shard_map/ppermute | solution.py:254
  6.8 2.6 %collective-permute-start.2 = (bf16[40,3072]{1,0:T(8,128)(2,1)}, bf16[40,3072]{1,0:T(8,128)(2,1)S(1)}, u32[]{:S(2)}, u32[]{:S(2)}) collective-permute-start(bf16[40,3072]{1,0:T(8,128)(2,1)} %refs_4_.1), channel_id=1, source_target_pairs={{0,8},{8,16},{16,24},{24,32},{32,40},{40,48},{48,56},{56,0},{1,9},... | collective-permute-start | bytes 737288 | tf_op jit(solution)/shard_map/ppermute | solution.py:254
  9.3 3.8 %collective-permute-start.3 = (bf16[40,3072]{1,0:T(8,128)(2,1)}, bf16[40,3072]{1,0:T(8,128)(2,1)S(1)}, u32[]{:S(2)}, u32[]{:S(2)}) collective-permute-start(bf16[40,3072]{1,0:T(8,128)(2,1)} %refs_4_.1), channel_id=1, source_target_pairs={{0,56},{8,0},{16,8},{24,16},{32,24},{40,32},{48,40},{56,48},{1,57}... | collective-permute-start | bytes 737288 | tf_op jit(solution)/shard_map/ppermute | solution.py:254
  15.2 2.8 %shard_map.136 = f32[12,5,384]{2,1,0:T(8,128)} custom-call(s32[1]{0:T(128)} %bitcast.rank, f32[2,12,256]{2,1,0:T(8,128)} %pad_maximum_fusion.1.conditions, bf16[256,384]{1,0:T(8,128)(2,1)} %shift.1, bf16[256,384]{1,0:T(8,128)(2,1)} %scale.1, bf16[256,384]{1,0:T(8,128)(2,1)} %gate.1), custom_call_target="tpu_custom_call" | custom-call | flops 1000000000 | bytes 1000000 | tf_op jit(solution)/shard_map/pallas_call | solution.py:33
  18.0 15.2 %all-to-all-start = ((f32[12,5,384]{2,1,0:T(8,128)}), f32[12,5,384]{2,1,0:T(8,128)S(1)}, u32[]{:S(2)}, u32[]{:S(2)}) async-start(f32[12,5,384]{2,1,0:T(8,128)} %shard_map.136), calls=%async_computation | async-start | bytes 294912 | tf_op jit(solution)/shard_map/all_to_all | solution.py:248
  36.5 3.9 %collective-permute-start.6 = (bf16[40,3072]{1,0:T(8,128)(2,1)}, bf16[40,3072]{1,0:T(8,128)(2,1)S(1)}, u32[]{:S(2)}, u32[]{:S(2)}) collective-permute-start(bf16[40,3072]{1,0:T(8,128)(2,1)} %broadcast_select_fusion), channel_id=1, source_target_pairs={{0,16},{1,49},{2,18},{3,51},{4,20},{5,53},{6,22},{7,55},{8,24},{9,... | collective-permute-start | bytes 737288 | tf_op jit(solution)/shard_map/ppermute | solution.py:271
  40.4 2.1 %collective-permute-start.1 = (bf16[40,3072]{1,0:T(8,128)(2,1)S(1)}, bf16[40,3072]{1,0:T(8,128)(2,1)S(1)}, u32[]{:S(2)}, u32[]{:S(2)}) collective-permute-start(bf16[40,3072]{1,0:T(8,128)(2,1)S(1)} %collective-permute-done.refs_2_), channel_id=1, source_target_pairs={{0,8},{8,16},{16,24},{24,32},{32,40},{40,48},{48,56},{56,0},{1,9},... | collective-permute-start | bytes 737288 | tf_op jit(solution)/shard_map/ppermute | solution.py:254
  42.6 3.7 %collective-permute-start.5 = (bf16[40,3072]{1,0:T(8,128)(2,1)S(1)}, bf16[40,3072]{1,0:T(8,128)(2,1)S(1)}, u32[]{:S(2)}, u32[]{:S(2)}) collective-permute-start(bf16[40,3072]{1,0:T(8,128)(2,1)S(1)} %collective-permute-done.4.refs_6_), channel_id=1, source_target_pairs={{0,56},{8,0},{16,8},{24,16},{32,24},{40,32},{48,40},{56,48},{1,57}... | collective-permute-start | bytes 737288 | tf_op jit(solution)/shard_map/ppermute | solution.py:254
  47.0 8.2 %all-to-all-start.1 = ((f32[8,5,384]{2,1,0:T(8,128)}), f32[8,5,384]{2,1,0:T(8,128)S(1)}, u32[]{:S(2)}, u32[]{:S(2)}) async-start(f32[8,5,384]{2,1,0:T(8,128)} %shard_map.137), calls=%async_computation.1 | async-start | bytes 196608 | tf_op jit(solution)/shard_map/all_to_all | solution.py:248
  55.2 4.9 %all-to-all-done.1.refs_9_.vectors = f32[8,5,384]{2,1,0:T(8,128)S(1)} async-done(((f32[8,5,384]{2,1,0:T(8,128)}), f32[8,5,384]{2,1,0:T(8,128)S(1)}, u32[]{:S(2)}, u32[]{:S(2)}) %all-to-all-start.1) | async-done | bytes 61472 | tf_op jit(solution)/shard_map/all_to_all | solution.py:248
  61.2 9.6 %all-to-all-start.2 = ((bf16[12,32,128]{2,1,0:T(8,128)(2,1)}), bf16[12,32,128]{2,1,0:T(8,128)(2,1)S(1)}, u32[]{:S(2)}, u32[]{:S(2)}) async-start(bf16[12,32,128]{2,1,0:T(8,128)(2,1)} %shard_map.140), calls=%async_computation.2 | async-start | bytes 196608 | tf_op jit(solution)/shard_map/all_to_all | solution.py:248
  70.9 2.0 %shard_map.138 = (bf16[320,3072]{1,0:T(8,128)(2,1)S(1)}, bf16[320,128]{1,0:T(8,128)(2,1)S(1)}, bf16[128,128]{1,0:T(8,128)(2,1)S(1)}, bf16[128,128]{1,0:T(8,128)(2,1)S(1)}) custom-call(s32[10]{0:T(128)S(1)} %pad_add_fusion.refs_0_.place, bf16[40,3072]{1,0:T(8,128)(2,1)S(1)} %collective-permute-done.1.refs_1_, ...), custom_call_target="tpu_custom_call" | custom-call | flops 1000000000 | bytes 1000000 | tf_op jit(solution)/shard_map/pallas_call | solution.py:33
  73.6 3.9 %collective-permute-start.7 = (bf16[128,128]{1,0:T(8,128)(2,1)S(1)}, bf16[128,128]{1,0:T(8,128)(2,1)S(1)}, u32[]{:S(2)}, u32[]{:S(2)}) collective-permute-start(bf16[128,128]{1,0:T(8,128)(2,1)S(1)} %get-tuple-element.14), channel_id=1, source_target_pairs={{0,64},{64,128},{128,192},{192,256},{256,320},{320,384},{384,448},... | collective-permute-start | bytes 98312 | tf_op jit(solution)/shard_map/ppermute | solution.py:254
  79.0 2.9 %shard_map.139 = (f32[1920,128]{1,0:T(8,128)S(1)}, f32[320,384]{1,0:T(8,128)S(1)}) custom-call(bf16[320,3072]{1,0:T(8,128)(2,1)S(1)} %get-tuple-element.11.hidden, bf16[3072,384]{1,0:T(8,128)(2,1)S(1)} %copy-done.1, bf16[3072,384]{1,0:T(8,128)(2,1)} %w_gate.1, f32[320,128]{1,0:T(8,128)S(1)} %get-tuple-element.25.refs_12_.cosine, ...), custom_call_target="tpu_custom_call" | custom-call | flops 2000000000 | bytes 1000000 | tf_op jit(solution)/shard_map/pallas_call | solution.py:33
  83.3 8.5 %shard_map.141 = bf16[320,3072]{1,0:T(8,128)(2,1)S(1)} custom-call(s32[10]{0:T(128)S(1)} %pad_add_fusion.refs_0_.place, f32[6]{0:T(128)S(1)} %copy-done.4, f32[1920,128]{1,0:T(8,128)S(1)} %get-tuple-element.12.queries, f32[320,384]{1,0:T(8,128)S(1)} %get-tuple-element.13.gate, bf16[128,128]{1,0:T(8,128)(2,1)S(1)} %collective-permute-done.7.low, ...), custom_call_target="tpu_custom_call" | custom-call | flops 3000000000 | bytes 1000000 | tf_op jit(solution)/shard_map/pallas_call | solution.py:33
  92.0 3.0 %collective-permute-start.11 = (bf16[40,3072]{1,0:T(8,128)(2,1)S(1)}, bf16[40,3072]{1,0:T(8,128)(2,1)S(1)}, u32[]{:S(2)}, u32[]{:S(2)}) collective-permute-start(bf16[40,3072]{1,0:T(8,128)(2,1)S(1)} %get-tuple-element.22), channel_id=1, source_target_pairs={{0,8},{8,16},{16,24},{24,32},{32,40},{40,48},{48,56},{56,0},{1,9},... | collective-permute-start | bytes 737288 | tf_op jit(solution)/shard_map/ppermute | solution.py:254
  95.0 5.1 %collective-permute-start.12 = (bf16[40,3072]{1,0:T(8,128)(2,1)S(1)}, bf16[40,3072]{1,0:T(8,128)(2,1)S(1)}, u32[]{:S(2)}, u32[]{:S(2)}) collective-permute-start(bf16[40,3072]{1,0:T(8,128)(2,1)S(1)} %get-tuple-element.21), channel_id=1, source_target_pairs={{0,16},{1,49},{2,18},{3,51},{4,20},{5,53},{6,22},{7,55},{8,24},{9,... | collective-permute-start | bytes 737288 | tf_op jit(solution)/shard_map/ppermute | solution.py:271
  100.1 3.4 %collective-permute-start.14 = (bf16[40,3072]{1,0:T(8,128)(2,1)S(1)}, bf16[40,3072]{1,0:T(8,128)(2,1)S(1)}, u32[]{:S(2)}, u32[]{:S(2)}) collective-permute-start(bf16[40,3072]{1,0:T(8,128)(2,1)S(1)} %get-tuple-element.20), channel_id=1, source_target_pairs={{0,56},{8,0},{16,8},{24,16},{32,24},{40,32},{48,40},{56,48},{1,57}... | collective-permute-start | bytes 737288 | tf_op jit(solution)/shard_map/ppermute | solution.py:254
  103.5 1.9 %collective-permute-start.10 = (bf16[40,3072]{1,0:T(8,128)(2,1)S(1)}, bf16[40,3072]{1,0:T(8,128)(2,1)S(1)}, u32[]{:S(2)}, u32[]{:S(2)}) collective-permute-start(bf16[40,3072]{1,0:T(8,128)(2,1)S(1)} %get-tuple-element.23), channel_id=1, source_target_pairs={{0,56},{8,0},{16,8},{24,16},{32,24},{40,32},{48,40},{56,48},{1,57}... | collective-permute-start | bytes 737288 | tf_op jit(solution)/shard_map/ppermute | solution.py:254
  105.4 3.9 %collective-permute-start.9 = (bf16[40,3072]{1,0:T(8,128)(2,1)S(1)}, bf16[40,3072]{1,0:T(8,128)(2,1)S(1)}, u32[]{:S(2)}, u32[]{:S(2)}) collective-permute-start(bf16[40,3072]{1,0:T(8,128)(2,1)S(1)} %get-tuple-element.19), channel_id=1, source_target_pairs={{0,8},{8,16},{16,24},{24,32},{32,40},{40,48},{48,56},{56,0},{1,9},... | collective-permute-start | bytes 737288 | tf_op jit(solution)/shard_map/ppermute | solution.py:254
  109.5 5.7 %collective-permute-start.13 = (bf16[40,3072]{1,0:T(8,128)(2,1)S(1)}, bf16[40,3072]{1,0:T(8,128)(2,1)S(1)}, u32[]{:S(2)}, u32[]{:S(2)}) collective-permute-start(bf16[40,3072]{1,0:T(8,128)(2,1)S(1)} %get-tuple-element.17), channel_id=1, source_target_pairs={{0,16},{8,24},{16,32},{24,40},{32,48},{40,56},{48,0},{56,8},{1,17}... | collective-permute-start | bytes 737288 | tf_op jit(solution)/shard_map/ppermute | solution.py:254
  115.2 1.9 %collective-permute-start.15 = (bf16[40,3072]{1,0:T(8,128)(2,1)S(1)}, bf16[40,3072]{1,0:T(8,128)(2,1)S(1)}, u32[]{:S(2)}, u32[]{:S(2)}) collective-permute-start(bf16[40,3072]{1,0:T(8,128)(2,1)S(1)} %get-tuple-element.18), channel_id=1, source_target_pairs={{0,48},{8,56},{16,0},{24,8},{32,16},{40,24},{48,32},{56,40},{1,49}... | collective-permute-start | bytes 737288 | tf_op jit(solution)/shard_map/ppermute | solution.py:254
  117.5 5.1 %collective-permute-done.13 = bf16[40,3072]{1,0:T(8,128)(2,1)S(1)} collective-permute-done((bf16[40,3072]{1,0:T(8,128)(2,1)S(1)}, bf16[40,3072]{1,0:T(8,128)(2,1)S(1)}, u32[]{:S(2)}, u32[]{:S(2)}) %collective-permute-start.13) | collective-permute-done | bytes 245792 | tf_op jit(solution)/shard_map/ppermute | solution.py:254
  122.6 4.9 %collective-permute-done.15 = bf16[40,3072]{1,0:T(8,128)(2,1)S(1)} collective-permute-done((bf16[40,3072]{1,0:T(8,128)(2,1)S(1)}, bf16[40,3072]{1,0:T(8,128)(2,1)S(1)}, u32[]{:S(2)}, u32[]{:S(2)}) %collective-permute-start.15) | collective-permute-done | bytes 245792 | tf_op jit(solution)/shard_map/ppermute | solution.py:254
  (51 shorter events, 14.0 us)
Async XLA Ops:
  0.0 35.8 %collective-permute-start = (bf16[40,3072]{1,0:T(8,128)(2,1)}, bf16[40,3072]{1,0:T(8,128)(2,1)S(1)}, u32[]{:S(2)}, u32[]{:S(2)}) collective-permute-start(bf16[40,3072]{1,0:T(8,128)(2,1)} %refs_4_.1), channel_id=1, source_target_pairs={{0,16},{8,24},{16,32},{24,40},{32,48},{40,56},{48,0},{56,8},{1,17}... | collective-permute-start | bytes 737288 | tf_op jit(solution)/shard_map/ppermute | solution.py:254
  1.9 33.9 %collective-permute-start.4 = (bf16[40,3072]{1,0:T(8,128)(2,1)}, bf16[40,3072]{1,0:T(8,128)(2,1)S(1)}, u32[]{:S(2)}, u32[]{:S(2)}) collective-permute-start(bf16[40,3072]{1,0:T(8,128)(2,1)} %refs_4_.1), channel_id=1, source_target_pairs={{0,48},{8,56},{16,0},{24,8},{32,16},{40,24},{48,32},{56,40},{1,49}... | collective-permute-start | bytes 737288 | tf_op jit(solution)/shard_map/ppermute | solution.py:254
  6.8 64.1 %collective-permute-start.2 = (bf16[40,3072]{1,0:T(8,128)(2,1)}, bf16[40,3072]{1,0:T(8,128)(2,1)S(1)}, u32[]{:S(2)}, u32[]{:S(2)}) collective-permute-start(bf16[40,3072]{1,0:T(8,128)(2,1)} %refs_4_.1), channel_id=1, source_target_pairs={{0,8},{8,16},{16,24},{24,32},{32,40},{40,48},{48,56},{56,0},{1,9},... | collective-permute-start | bytes 737288 | tf_op jit(solution)/shard_map/ppermute | solution.py:254
  9.3 61.6 %collective-permute-start.3 = (bf16[40,3072]{1,0:T(8,128)(2,1)}, bf16[40,3072]{1,0:T(8,128)(2,1)S(1)}, u32[]{:S(2)}, u32[]{:S(2)}) collective-permute-start(bf16[40,3072]{1,0:T(8,128)(2,1)} %refs_4_.1), channel_id=1, source_target_pairs={{0,56},{8,0},{16,8},{24,16},{32,24},{40,32},{48,40},{56,48},{1,57}... | collective-permute-start | bytes 737288 | tf_op jit(solution)/shard_map/ppermute | solution.py:254
  18.0 28.3 %all-to-all-start = ((f32[12,5,384]{2,1,0:T(8,128)}), f32[12,5,384]{2,1,0:T(8,128)S(1)}, u32[]{:S(2)}, u32[]{:S(2)}) async-start(f32[12,5,384]{2,1,0:T(8,128)} %shard_map.136), calls=%async_computation | async-start | bytes 294912 | tf_op jit(solution)/shard_map/all_to_all | solution.py:248
  36.5 23.6 %copy-start.2 = (bf16[32,3072]{1,0:T(8,128)(2,1)S(1)}, bf16[32,3072]{1,0:T(8,128)(2,1)}, u32[]{:S(2)}) copy-start(bf16[32,3072]{1,0:T(8,128)(2,1)} %context.1) | copy-start | bytes 589828
  36.5 23.6 %copy-start.3 = (f32[3072]{0:T(1024)S(1)}, f32[3072]{0:T(1024)}, u32[]{:S(2)}) copy-start(f32[3072]{0:T(1024)} %param.21) | copy-start | bytes 36868
  36.5 34.4 %collective-permute-start.6 = (bf16[40,3072]{1,0:T(8,128)(2,1)}, bf16[40,3072]{1,0:T(8,128)(2,1)S(1)}, u32[]{:S(2)}, u32[]{:S(2)}) collective-permute-start(bf16[40,3072]{1,0:T(8,128)(2,1)} %broadcast_select_fusion), channel_id=1, source_target_pairs={{0,16},{1,49},{2,18},{3,51},{4,20},{5,53},{6,22},{7,55},{8,24},{9,... | collective-permute-start | bytes 737288 | tf_op jit(solution)/shard_map/ppermute | solution.py:271
  40.4 30.5 %collective-permute-start.1 = (bf16[40,3072]{1,0:T(8,128)(2,1)S(1)}, bf16[40,3072]{1,0:T(8,128)(2,1)S(1)}, u32[]{:S(2)}, u32[]{:S(2)}) collective-permute-start(bf16[40,3072]{1,0:T(8,128)(2,1)S(1)} %collective-permute-done.refs_2_), channel_id=1, source_target_pairs={{0,8},{8,16},{16,24},{24,32},{32,40},{40,48},{48,56},{56,0},{1,9},... | collective-permute-start | bytes 737288 | tf_op jit(solution)/shard_map/ppermute | solution.py:254
  42.6 28.3 %collective-permute-start.5 = (bf16[40,3072]{1,0:T(8,128)(2,1)S(1)}, bf16[40,3072]{1,0:T(8,128)(2,1)S(1)}, u32[]{:S(2)}, u32[]{:S(2)}) collective-permute-start(bf16[40,3072]{1,0:T(8,128)(2,1)S(1)} %collective-permute-done.4.refs_6_), channel_id=1, source_target_pairs={{0,56},{8,0},{16,8},{24,16},{32,24},{40,32},{48,40},{56,48},{1,57}... | collective-permute-start | bytes 737288 | tf_op jit(solution)/shard_map/ppermute | solution.py:254
  47.0 13.2 %all-to-all-start.1 = ((f32[8,5,384]{2,1,0:T(8,128)}), f32[8,5,384]{2,1,0:T(8,128)S(1)}, u32[]{:S(2)}, u32[]{:S(2)}) async-start(f32[8,5,384]{2,1,0:T(8,128)} %shard_map.137), calls=%async_computation.1 | async-start | bytes 196608 | tf_op jit(solution)/shard_map/all_to_all | solution.py:248
  55.2 15.8 %copy-start = (bf16[40,3072]{1,0:T(8,128)(2,1)S(1)}, bf16[40,3072]{1,0:T(8,128)(2,1)}, u32[]{:S(2)}) copy-start(bf16[40,3072]{1,0:T(8,128)(2,1)} %refs_4_.1) | copy-start | bytes 737284
  61.2 22.1 %all-to-all-start.2 = ((bf16[12,32,128]{2,1,0:T(8,128)(2,1)}), bf16[12,32,128]{2,1,0:T(8,128)(2,1)S(1)}, u32[]{:S(2)}, u32[]{:S(2)}) async-start(bf16[12,32,128]{2,1,0:T(8,128)(2,1)} %shard_map.140), calls=%async_computation.2 | async-start | bytes 196608 | tf_op jit(solution)/shard_map/all_to_all | solution.py:248
  70.9 8.1 %copy-start.1 = (bf16[3072,384]{1,0:T(8,128)(2,1)S(1)}, bf16[3072,384]{1,0:T(8,128)(2,1)}, u32[]{:S(2)}) copy-start(bf16[3072,384]{1,0:T(8,128)(2,1)} %w_query.1) | copy-start | bytes 7077892
  73.6 8.3 %collective-permute-start.7 = (bf16[128,128]{1,0:T(8,128)(2,1)S(1)}, bf16[128,128]{1,0:T(8,128)(2,1)S(1)}, u32[]{:S(2)}, u32[]{:S(2)}) collective-permute-start(bf16[128,128]{1,0:T(8,128)(2,1)S(1)} %get-tuple-element.14), channel_id=1, source_target_pairs={{0,64},{64,128},{128,192},{192,256},{256,320},{320,384},{384,448},... | collective-permute-start | bytes 98312 | tf_op jit(solution)/shard_map/ppermute | solution.py:254
  77.5 5.8 %collective-permute-start.8 = (bf16[128,128]{1,0:T(8,128)(2,1)S(1)}, bf16[128,128]{1,0:T(8,128)(2,1)S(1)}, u32[]{:S(2)}, u32[]{:S(2)}) collective-permute-start(bf16[128,128]{1,0:T(8,128)(2,1)S(1)} %get-tuple-element.16), channel_id=1, source_target_pairs={{64,0},{128,64},{192,128},{256,192},{320,256},{384,320},{448,384},... | collective-permute-start | bytes 98312 | tf_op jit(solution)/shard_map/ppermute | solution.py:254
  79.0 4.3 %copy-start.4 = (f32[6]{0:T(128)S(1)}, f32[6]{0:T(128)}, u32[]{:S(2)}) copy-start(f32[6]{0:T(128)} %sink.1) | copy-start | bytes 76
  92.0 17.4 %collective-permute-start.11 = (bf16[40,3072]{1,0:T(8,128)(2,1)S(1)}, bf16[40,3072]{1,0:T(8,128)(2,1)S(1)}, u32[]{:S(2)}, u32[]{:S(2)}) collective-permute-start(bf16[40,3072]{1,0:T(8,128)(2,1)S(1)} %get-tuple-element.22), channel_id=1, source_target_pairs={{0,8},{8,16},{16,24},{24,32},{32,40},{40,48},{48,56},{56,0},{1,9},... | collective-permute-start | bytes 737288 | tf_op jit(solution)/shard_map/ppermute | solution.py:254
  95.0 14.4 %collective-permute-start.12 = (bf16[40,3072]{1,0:T(8,128)(2,1)S(1)}, bf16[40,3072]{1,0:T(8,128)(2,1)S(1)}, u32[]{:S(2)}, u32[]{:S(2)}) collective-permute-start(bf16[40,3072]{1,0:T(8,128)(2,1)S(1)} %get-tuple-element.21), channel_id=1, source_target_pairs={{0,16},{1,49},{2,18},{3,51},{4,20},{5,53},{6,22},{7,55},{8,24},{9,... | collective-permute-start | bytes 737288 | tf_op jit(solution)/shard_map/ppermute | solution.py:271
  100.1 9.3 %collective-permute-start.14 = (bf16[40,3072]{1,0:T(8,128)(2,1)S(1)}, bf16[40,3072]{1,0:T(8,128)(2,1)S(1)}, u32[]{:S(2)}, u32[]{:S(2)}) collective-permute-start(bf16[40,3072]{1,0:T(8,128)(2,1)S(1)} %get-tuple-element.20), channel_id=1, source_target_pairs={{0,56},{8,0},{16,8},{24,16},{32,24},{40,32},{48,40},{56,48},{1,57}... | collective-permute-start | bytes 737288 | tf_op jit(solution)/shard_map/ppermute | solution.py:254
  103.5 13.7 %collective-permute-start.10 = (bf16[40,3072]{1,0:T(8,128)(2,1)S(1)}, bf16[40,3072]{1,0:T(8,128)(2,1)S(1)}, u32[]{:S(2)}, u32[]{:S(2)}) collective-permute-start(bf16[40,3072]{1,0:T(8,128)(2,1)S(1)} %get-tuple-element.23), channel_id=1, source_target_pairs={{0,56},{8,0},{16,8},{24,16},{32,24},{40,32},{48,40},{56,48},{1,57}... | collective-permute-start | bytes 737288 | tf_op jit(solution)/shard_map/ppermute | solution.py:254
  105.4 12.1 %collective-permute-start.9 = (bf16[40,3072]{1,0:T(8,128)(2,1)S(1)}, bf16[40,3072]{1,0:T(8,128)(2,1)S(1)}, u32[]{:S(2)}, u32[]{:S(2)}) collective-permute-start(bf16[40,3072]{1,0:T(8,128)(2,1)S(1)} %get-tuple-element.19), channel_id=1, source_target_pairs={{0,8},{8,16},{16,24},{24,32},{32,40},{40,48},{48,56},{56,0},{1,9},... | collective-permute-start | bytes 737288 | tf_op jit(solution)/shard_map/ppermute | solution.py:254
  109.5 13.1 %collective-permute-start.13 = (bf16[40,3072]{1,0:T(8,128)(2,1)S(1)}, bf16[40,3072]{1,0:T(8,128)(2,1)S(1)}, u32[]{:S(2)}, u32[]{:S(2)}) collective-permute-start(bf16[40,3072]{1,0:T(8,128)(2,1)S(1)} %get-tuple-element.17), channel_id=1, source_target_pairs={{0,16},{8,24},{16,32},{24,40},{32,48},{40,56},{48,0},{56,8},{1,17}... | collective-permute-start | bytes 737288 | tf_op jit(solution)/shard_map/ppermute | solution.py:254
  115.2 12.2 %collective-permute-start.15 = (bf16[40,3072]{1,0:T(8,128)(2,1)S(1)}, bf16[40,3072]{1,0:T(8,128)(2,1)S(1)}, u32[]{:S(2)}, u32[]{:S(2)}) collective-permute-start(bf16[40,3072]{1,0:T(8,128)(2,1)S(1)} %get-tuple-element.18), channel_id=1, source_target_pairs={{0,48},{8,56},{16,0},{24,8},{32,16},{40,24},{48,32},{56,40},{1,49}... | collective-permute-start | bytes 737288 | tf_op jit(solution)/shard_map/ppermute | solution.py:254
  (2 other events, 5.0 us)

commit v5 on v4

--- a/solution.py
+++ b/solution.py
@@ -41,13 +41,13 @@
     )(*operands)
 
 
-def partial_kernel(rank, conditions, shift, scale, gate, out, held, ready):
+def partial_kernel(rank, condition, ctx_condition, shift, scale, gate, out, held, ready):
     fetches = []
     for index, weight in enumerate((shift, scale, gate)):
         fetches.append(pltpu.make_async_copy(weight, held.at[index], ready.at[index]))
         fetches[-1].start()
-    mine = pl.ds(rank[0], 1)
-    values = jnp.concatenate([conditions[0, mine, :], conditions[1, mine, :]], axis=0)
+    mine = pl.ds(pl.multiple_of(rank[0] * held.shape[1], held.shape[1]), held.shape[1])
+    values = jnp.stack([condition[mine], ctx_condition[mine]])
     acts = rounded(values / (1.0 + jnp.exp(-values)))
     sums = []
     for index, fetch in enumerate(fetches):
@@ -261,7 +261,7 @@
     return rounded(total)
 
 
-def shift_by_parity(block, steps):
+def toward(block, steps):
     tp_count, dp_count = lax.axis_size("tp"), lax.axis_size("dp")
     pairs = []
     for i in range(tp_count):
@@ -271,22 +271,24 @@
     return lax.ppermute(block, ("tp", "dp"), pairs)
 
 
-def gather_rows(latent, even):
-    low2, high2 = shift(latent, "tp", 2), shift(latent, "tp", -2)
-    low1, high1 = shift(latent, "tp", 1), shift(latent, "tp", -1)
-    far = shift_by_parity(jnp.where(even, low2, high2), 2)
-    low3, high3 = shift(low2, "tp", 1), shift(high2, "tp", -1)
-    return [(low3,), (low2,), (low1,), (latent,), (high1,), (high2,), (high3,), (far,)]
-
-
-def reduce_rows(block, even):
-    far = shift_by_parity(block(4), 2)
-    up3, down3 = shift(block(3), "tp", 1), shift(block(-3), "tp", -1)
-    nothing = jnp.zeros_like(far)
-    two = added(block(2), up3, jnp.where(even, far, nothing))
-    minus_two = added(block(-2), down3, jnp.where(even, nothing, far))
-    up2, down2 = shift(two, "tp", 2), shift(minus_two, "tp", -2)
-    up1, down1 = shift(block(1), "tp", 1), shift(block(-1), "tp", -1)
+def gather_rows(latent):
+    back2 = toward(latent, 2)
+    ahead2 = toward(latent, -2)
+    back1, ahead1 = toward(latent, 1), toward(latent, -1)
+    far = toward(back2, 2)
+    back3, ahead3 = toward(back2, 1), toward(ahead2, -1)
+    return [(back3,), (back2,), (back1,), (latent,), (ahead1,), (ahead2,), (ahead3,), (far,)]
+
+
+def reduce_rows(block):
+    far = toward(block(4), 2)
+    down3 = toward(block(-3), -1)
+    up3 = toward(block(3), 1)
+    minus_two = added(block(-2), down3)
+    down2 = toward(minus_two, -2)
+    ahead, _ = lax.optimization_barrier((block(2), minus_two))
+    up2 = toward(added(ahead, up3, far), 2)
+    up1, down1 = toward(block(1), 1), toward(block(-1), -1)
     total = block(0).astype(jnp.float32)
     for part in (up1, down1, up2, down2):
         total = total + part.astype(jnp.float32)
@@ -331,30 +333,29 @@
     mod_rows, columns = mod_shift.shape
     behind = (tp_count - 1) // 2
 
-    conditions = jnp.stack([condition, ctx_condition]).reshape(2, sp_count, mod_rows)
     parts = call(
         partial_kernel,
         shape((sp_count, 5, columns), f32),
         sp_rank.astype(jnp.int32)[None],
-        conditions,
+        condition,
+        ctx_condition,
         mod_shift,
         mod_scale,
         mod_gate,
-        specs=[SMEM, VMEM, HBM, HBM, HBM],
+        specs=[SMEM, VMEM, VMEM, HBM, HBM, HBM],
         scratch=[pltpu.VMEM((3, mod_rows, columns), bf16), pltpu.SemaphoreType.DMA((3,))],
         grant=63,
     )
-    even = lax.axis_index("dp") % 2 == 0
-    pieces = gather_rows(latent, even)
+    pieces = gather_rows(latent)
     parts = copy_for_each(parts, "sp")
     totals = call(total_kernel, shape((tp_count, 5, columns), f32), parts)
     vectors = copy_for_each(totals, "tp")
 
     gain = norm_gain[None, :]
     kv_weight = jnp.concatenate([key_weight.T, value_weight.T], axis=0)
-    offsets = (
-        (tp_rank + tp_count - behind + jnp.arange(tp_count, dtype=jnp.int32)) % tp_count * own
-    )
+    direction = 1 - 2 * (lax.axis_index("dp") % 2)
+    distance = jnp.arange(-behind, tp_count - behind, dtype=jnp.int32)
+    offsets = (tp_rank + tp_count + direction * distance) % tp_count * own
     begin = sp_rank * rows
     positions = begin + (offsets[:, None] + jnp.arange(own, dtype=jnp.int32)).reshape(rows)
     cosine, sine = angle_tables(positions)
@@ -430,7 +431,7 @@
         flops=3 * 10**9,
         grant=50,
     )
-    branch = reduce_rows(lambda d: product[(d + behind) * own : (d + behind + 1) * own], even)
+    branch = reduce_rows(lambda d: product[(d + behind) * own : (d + behind + 1) * own])
     lat_gate = vectors[:, 4, :].reshape(width)
     return rounded(latent.astype(f32) + lat_gate * branch)
 

time: 129 us -> 128 us (level)
  the two profiles are of different devices: /device:TPU:50 before, /device:TPU:26 now
where the time goes in v5:
time: 128 us; the launch traced here: 127 us
  starting transfers between devices  84.6 us (66%)
  waiting for transfers between devices  20 us (16%)
  Pallas kernels  18 us (14%)
  other arithmetic  3.56 us (3%)
    ppermute x14, starting transfers between devices, toward(): return lax.ppermute(block, ('tp', 'dp'), pairs)  48.2 us
    all_to_all x3, starting transfers between devices, copy_for_each(): return lax.all_to_all(copies, axis, split_axis=0, concat_axis=0, tiled=True)  31.1 us
    pallas_call x6, Pallas kernels, call(): pl.pallas_call(kernel, out_shape=out_shape, in_specs=specs or [VMEM] * le...  18 us
    ppermute x14, waiting for transfers between devices, toward(): return lax.ppermute(block, ('tp', 'dp'), pairs)  13.5 us
    ppermute x2, starting transfers between devices, shift(): return lax.ppermute(block, axis, pairs)  5.34 us
    all_to_all x3, waiting for transfers between devices, copy_for_each(): return lax.all_to_all(copies, axis, split_axis=0, concat_axis=0, tiled=True)  5.14 us
  transfers between devices with their start and end apart: 19, of which 5 were waited for; matrix products, arithmetic and copies ran while one was open for 2% of the time, Pallas kernels for 7%

profile of v5, /device:TPU:26, one launch (start us, length us, event | category | flops | bytes accessed | tf_op | source)
XLA Modules:
  0.0 127.5 jit_solution(15580455555436594946)
XLA Ops:
  0.0 4.8 %collective-permute-start = (bf16[40,3072]{1,0:T(8,128)(2,1)}, bf16[40,3072]{1,0:T(8,128)(2,1)S(1)}, u32[]{:S(2)}, u32[]{:S(2)}) collective-permute-start(bf16[40,3072]{1,0:T(8,128)(2,1)} %refs_4_.1), channel_id=1, source_target_pairs={{0,16},{1,49},{2,18},{3,51},{4,20},{5,53},{6,22},{7,55},{8,24},{9,... | collective-permute-start | bytes 737288 | tf_op jit(solution)/shard_map/ppermute | solution.py:271
  4.8 1.9 %collective-permute-start.4 = (bf16[40,3072]{1,0:T(8,128)(2,1)}, bf16[40,3072]{1,0:T(8,128)(2,1)S(1)}, u32[]{:S(2)}, u32[]{:S(2)}) collective-permute-start(bf16[40,3072]{1,0:T(8,128)(2,1)} %refs_4_.1), channel_id=1, source_target_pairs={{0,48},{1,17},{2,50},{3,19},{4,52},{5,21},{6,54},{7,23},{8,56},{9,... | collective-permute-start | bytes 737288 | tf_op jit(solution)/shard_map/ppermute | solution.py:271
  6.8 5.9 %collective-permute-start.2 = (bf16[40,3072]{1,0:T(8,128)(2,1)}, bf16[40,3072]{1,0:T(8,128)(2,1)S(1)}, u32[]{:S(2)}, u32[]{:S(2)}) collective-permute-start(bf16[40,3072]{1,0:T(8,128)(2,1)} %refs_4_.1), channel_id=1, source_target_pairs={{0,8},{1,57},{2,10},{3,59},{4,12},{5,61},{6,14},{7,63},{8,16},{9,1... | collective-permute-start | bytes 737288 | tf_op jit(solution)/shard_map/ppermute | solution.py:271
  14.6 2.8 %shard_map.136 = f32[12,5,384]{2,1,0:T(8,128)} custom-call(s32[1]{0:T(128)} %bitcast.rank, f32[3072]{0:T(1024)} %condition.1, f32[3072]{0:T(1024)} %ctx_condition.1, bf16[256,384]{1,0:T(8,128)(2,1)} %shift.1, bf16[256,384]{1,0:T(8,128)(2,1)} %scale.1, bf16[256,384]{1,0:T(8,128)(2,1)} %gate.1), custom_call_target="tpu_custom_call" | custom-call | flops 1000000000 | bytes 1000000 | tf_op jit(solution)/shard_map/pallas_call | solution.py:33
  17.4 15.2 %all-to-all-start = ((f32[12,5,384]{2,1,0:T(8,128)}), f32[12,5,384]{2,1,0:T(8,128)S(1)}, u32[]{:S(2)}, u32[]{:S(2)}) async-start(f32[12,5,384]{2,1,0:T(8,128)} %shard_map.136), calls=%async_computation | async-start | bytes 294912 | tf_op jit(solution)/shard_map/all_to_all | solution.py:248
  35.2 5.3 %collective-permute-start.1 = (bf16[40,3072]{1,0:T(8,128)(2,1)S(1)}, bf16[40,3072]{1,0:T(8,128)(2,1)S(1)}, u32[]{:S(2)}, u32[]{:S(2)}) collective-permute-start(bf16[40,3072]{1,0:T(8,128)(2,1)S(1)} %collective-permute-done.refs_2_), channel_id=1, source_target_pairs={{0,8},{1,57},{2,10},{3,59},{4,12},{5,61},{6,14},{7,63},{8,16},{9,1... | collective-permute-start | bytes 737288 | tf_op jit(solution)/shard_map/ppermute | solution.py:271
  42.4 3.4 %collective-permute-start.5 = (bf16[40,3072]{1,0:T(8,128)(2,1)S(1)}, bf16[40,3072]{1,0:T(8,128)(2,1)S(1)}, u32[]{:S(2)}, u32[]{:S(2)}) collective-permute-start(bf16[40,3072]{1,0:T(8,128)(2,1)S(1)} %collective-permute-done.4.refs_6_), channel_id=1, source_target_pairs={{0,56},{1,9},{2,58},{3,11},{4,60},{5,13},{6,62},{7,15},{8,0},{9,17... | collective-permute-start | bytes 737288 | tf_op jit(solution)/shard_map/ppermute | solution.py:271
  46.4 6.4 %all-to-all-start.1 = ((f32[8,5,384]{2,1,0:T(8,128)}), f32[8,5,384]{2,1,0:T(8,128)S(1)}, u32[]{:S(2)}, u32[]{:S(2)}) async-start(f32[8,5,384]{2,1,0:T(8,128)} %shard_map.137), calls=%async_computation.1 | async-start | bytes 196608 | tf_op jit(solution)/shard_map/all_to_all | solution.py:248
  53.0 5.1 %all-to-all-done.1.refs_9_.vectors = f32[8,5,384]{2,1,0:T(8,128)S(1)} async-done(((f32[8,5,384]{2,1,0:T(8,128)}), f32[8,5,384]{2,1,0:T(8,128)S(1)}, u32[]{:S(2)}, u32[]{:S(2)}) %all-to-all-start.1) | async-done | bytes 61472 | tf_op jit(solution)/shard_map/all_to_all | solution.py:248
  59.2 9.5 %all-to-all-start.2 = ((bf16[12,32,128]{2,1,0:T(8,128)(2,1)}), bf16[12,32,128]{2,1,0:T(8,128)(2,1)S(1)}, u32[]{:S(2)}, u32[]{:S(2)}) async-start(bf16[12,32,128]{2,1,0:T(8,128)(2,1)} %shard_map.140), calls=%async_computation.2 | async-start | bytes 196608 | tf_op jit(solution)/shard_map/all_to_all | solution.py:248
  68.7 2.0 %shard_map.138 = (bf16[320,3072]{1,0:T(8,128)(2,1)S(1)}, bf16[320,128]{1,0:T(8,128)(2,1)S(1)}, bf16[128,128]{1,0:T(8,128)(2,1)S(1)}, bf16[128,128]{1,0:T(8,128)(2,1)S(1)}) custom-call(s32[10]{0:T(128)S(1)} %pad_add_fusion.refs_0_.place, bf16[40,3072]{1,0:T(8,128)(2,1)S(1)} %collective-permute-done.1.refs_1_, ...), custom_call_target="tpu_custom_call" | custom-call | flops 1000000000 | bytes 1000000 | tf_op jit(solution)/shard_map/pallas_call | solution.py:33
  71.4 3.9 %collective-permute-start.7 = (bf16[128,128]{1,0:T(8,128)(2,1)S(1)}, bf16[128,128]{1,0:T(8,128)(2,1)S(1)}, u32[]{:S(2)}, u32[]{:S(2)}) collective-permute-start(bf16[128,128]{1,0:T(8,128)(2,1)S(1)} %get-tuple-element.15), channel_id=1, source_target_pairs={{0,64},{64,128},{128,192},{192,256},{256,320},{320,384},{384,448},... | collective-permute-start | bytes 98312 | tf_op jit(solution)/shard_map/ppermute | solution.py:254
  76.8 2.9 %shard_map.139 = (f32[1920,128]{1,0:T(8,128)S(1)}, f32[320,384]{1,0:T(8,128)S(1)}) custom-call(bf16[320,3072]{1,0:T(8,128)(2,1)S(1)} %get-tuple-element.12.hidden, bf16[3072,384]{1,0:T(8,128)(2,1)S(1)} %copy-done.1, bf16[3072,384]{1,0:T(8,128)(2,1)} %w_gate.1, f32[320,128]{1,0:T(8,128)S(1)} %get-tuple-element.26.refs_12_.cosine, ...), custom_call_target="tpu_custom_call" | custom-call | flops 2000000000 | bytes 1000000 | tf_op jit(solution)/shard_map/pallas_call | solution.py:33
  81.1 8.5 %shard_map.141 = bf16[320,3072]{1,0:T(8,128)(2,1)S(1)} custom-call(s32[10]{0:T(128)S(1)} %pad_add_fusion.refs_0_.place, f32[6]{0:T(128)S(1)} %copy-done.4, f32[1920,128]{1,0:T(8,128)S(1)} %get-tuple-element.13.queries, f32[320,384]{1,0:T(8,128)S(1)} %get-tuple-element.14.gate, bf16[128,128]{1,0:T(8,128)(2,1)S(1)} %collective-permute-done.7.low, ...), custom_call_target="tpu_custom_call" | custom-call | flops 3000000000 | bytes 1000000 | tf_op jit(solution)/shard_map/pallas_call | solution.py:33
  89.7 3.5 %collective-permute-start.11 = (bf16[40,3072]{1,0:T(8,128)(2,1)S(1)}, bf16[40,3072]{1,0:T(8,128)(2,1)S(1)}, u32[]{:S(2)}, u32[]{:S(2)}) collective-permute-start(bf16[40,3072]{1,0:T(8,128)(2,1)S(1)} %get-tuple-element.22), channel_id=1, source_target_pairs={{0,56},{1,9},{2,58},{3,11},{4,60},{5,13},{6,62},{7,15},{8,0},{9,17... | collective-permute-start | bytes 737288 | tf_op jit(solution)/shard_map/ppermute | solution.py:271
  93.2 3.6 %collective-permute-start.12 = (bf16[40,3072]{1,0:T(8,128)(2,1)S(1)}, bf16[40,3072]{1,0:T(8,128)(2,1)S(1)}, u32[]{:S(2)}, u32[]{:S(2)}) collective-permute-start(bf16[40,3072]{1,0:T(8,128)(2,1)S(1)} %get-tuple-element.21), channel_id=1, source_target_pairs={{0,8},{1,57},{2,10},{3,59},{4,12},{5,61},{6,14},{7,63},{8,16},{9,1... | collective-permute-start | bytes 737288 | tf_op jit(solution)/shard_map/ppermute | solution.py:271
  96.8 2.3 %collective-permute-start.13 = (bf16[40,3072]{1,0:T(8,128)(2,1)S(1)}, bf16[40,3072]{1,0:T(8,128)(2,1)S(1)}, u32[]{:S(2)}, u32[]{:S(2)}) collective-permute-start(bf16[40,3072]{1,0:T(8,128)(2,1)S(1)} %get-tuple-element.20), channel_id=1, source_target_pairs={{0,16},{1,49},{2,18},{3,51},{4,20},{5,53},{6,22},{7,55},{8,24},{9,... | collective-permute-start | bytes 737288 | tf_op jit(solution)/shard_map/ppermute | solution.py:271
  99.1 3.0 %collective-permute-start.10 = (bf16[40,3072]{1,0:T(8,128)(2,1)S(1)}, bf16[40,3072]{1,0:T(8,128)(2,1)S(1)}, u32[]{:S(2)}, u32[]{:S(2)}) collective-permute-start(bf16[40,3072]{1,0:T(8,128)(2,1)S(1)} %get-tuple-element.24), channel_id=1, source_target_pairs={{0,56},{1,9},{2,58},{3,11},{4,60},{5,13},{6,62},{7,15},{8,0},{9,17... | collective-permute-start | bytes 737288 | tf_op jit(solution)/shard_map/ppermute | solution.py:271
  102.1 4.0 %collective-permute-start.9 = (bf16[40,3072]{1,0:T(8,128)(2,1)S(1)}, bf16[40,3072]{1,0:T(8,128)(2,1)S(1)}, u32[]{:S(2)}, u32[]{:S(2)}) collective-permute-start(bf16[40,3072]{1,0:T(8,128)(2,1)S(1)} %get-tuple-element.19), channel_id=1, source_target_pairs={{0,8},{1,57},{2,10},{3,59},{4,12},{5,61},{6,14},{7,63},{8,16},{9,1... | collective-permute-start | bytes 737288 | tf_op jit(solution)/shard_map/ppermute | solution.py:271
  106.2 4.0 %collective-permute-done.13 = bf16[40,3072]{1,0:T(8,128)(2,1)S(1)} collective-permute-done((bf16[40,3072]{1,0:T(8,128)(2,1)S(1)}, bf16[40,3072]{1,0:T(8,128)(2,1)S(1)}, u32[]{:S(2)}, u32[]{:S(2)}) %collective-permute-start.13) | collective-permute-done | bytes 245792 | tf_op jit(solution)/shard_map/ppermute | solution.py:271
  110.4 3.9 %collective-permute-start.14 = (bf16[40,3072]{1,0:T(8,128)(2,1)S(1)}, bf16[40,3072]{1,0:T(8,128)(2,1)S(1)}, u32[]{:S(2)}, u32[]{:S(2)}) collective-permute-start(bf16[40,3072]{1,0:T(8,128)(2,1)S(1)} %add_convert_fusion.1), channel_id=1, source_target_pairs={{0,16},{1,49},{2,18},{3,51},{4,20},{5,53},{6,22},{7,55},{8,24},{9,... | collective-permute-start | bytes 737288 | tf_op jit(solution)/shard_map/ppermute | solution.py:271
  114.3 2.8 %collective-permute-start.15 = (bf16[40,3072]{1,0:T(8,128)(2,1)S(1)}, bf16[40,3072]{1,0:T(8,128)(2,1)S(1)}, u32[]{:S(2)}, u32[]{:S(2)}) collective-permute-start(bf16[40,3072]{1,0:T(8,128)(2,1)S(1)} %add_convert_fusion.2), channel_id=1, source_target_pairs={{0,48},{1,17},{2,50},{3,19},{4,52},{5,21},{6,54},{7,23},{8,56},{9,... | collective-permute-start | bytes 737288 | tf_op jit(solution)/shard_map/ppermute | solution.py:271
  117.2 6.1 %collective-permute-done.14 = bf16[40,3072]{1,0:T(8,128)(2,1)S(1)} collective-permute-done((bf16[40,3072]{1,0:T(8,128)(2,1)S(1)}, bf16[40,3072]{1,0:T(8,128)(2,1)S(1)}, u32[]{:S(2)}, u32[]{:S(2)}) %collective-permute-start.14) | collective-permute-done | bytes 245792 | tf_op jit(solution)/shard_map/ppermute | solution.py:271
  123.3 3.3 %collective-permute-done.15 = bf16[40,3072]{1,0:T(8,128)(2,1)S(1)} collective-permute-done((bf16[40,3072]{1,0:T(8,128)(2,1)S(1)}, bf16[40,3072]{1,0:T(8,128)(2,1)S(1)}, u32[]{:S(2)}, u32[]{:S(2)}) %collective-permute-start.15) | collective-permute-done | bytes 245792 | tf_op jit(solution)/shard_map/ppermute | solution.py:271
  (48 shorter events, 12.9 us)
Async XLA Ops:
  0.0 35.2 %collective-permute-start = (bf16[40,3072]{1,0:T(8,128)(2,1)}, bf16[40,3072]{1,0:T(8,128)(2,1)S(1)}, u32[]{:S(2)}, u32[]{:S(2)}) collective-permute-start(bf16[40,3072]{1,0:T(8,128)(2,1)} %refs_4_.1), channel_id=1, source_target_pairs={{0,16},{1,49},{2,18},{3,51},{4,20},{5,53},{6,22},{7,55},{8,24},{9,... | collective-permute-start | bytes 737288 | tf_op jit(solution)/shard_map/ppermute | solution.py:271
  4.8 37.6 %collective-permute-start.4 = (bf16[40,3072]{1,0:T(8,128)(2,1)}, bf16[40,3072]{1,0:T(8,128)(2,1)S(1)}, u32[]{:S(2)}, u32[]{:S(2)}) collective-permute-start(bf16[40,3072]{1,0:T(8,128)(2,1)} %refs_4_.1), channel_id=1, source_target_pairs={{0,48},{1,17},{2,50},{3,19},{4,52},{5,21},{6,54},{7,23},{8,56},{9,... | collective-permute-start | bytes 737288 | tf_op jit(solution)/shard_map/ppermute | solution.py:271
  6.8 61.9 %collective-permute-start.2 = (bf16[40,3072]{1,0:T(8,128)(2,1)}, bf16[40,3072]{1,0:T(8,128)(2,1)S(1)}, u32[]{:S(2)}, u32[]{:S(2)}) collective-permute-start(bf16[40,3072]{1,0:T(8,128)(2,1)} %refs_4_.1), channel_id=1, source_target_pairs={{0,8},{1,57},{2,10},{3,59},{4,12},{5,61},{6,14},{7,63},{8,16},{9,1... | collective-permute-start | bytes 737288 | tf_op jit(solution)/shard_map/ppermute | solution.py:271
  12.7 56.0 %collective-permute-start.3 = (bf16[40,3072]{1,0:T(8,128)(2,1)}, bf16[40,3072]{1,0:T(8,128)(2,1)S(1)}, u32[]{:S(2)}, u32[]{:S(2)}) collective-permute-start(bf16[40,3072]{1,0:T(8,128)(2,1)} %refs_4_.1), channel_id=1, source_target_pairs={{0,56},{1,9},{2,58},{3,11},{4,60},{5,13},{6,62},{7,15},{8,0},{9,17... | collective-permute-start | bytes 737288 | tf_op jit(solution)/shard_map/ppermute | solution.py:271
  17.4 28.4 %all-to-all-start = ((f32[12,5,384]{2,1,0:T(8,128)}), f32[12,5,384]{2,1,0:T(8,128)S(1)}, u32[]{:S(2)}, u32[]{:S(2)}) async-start(f32[12,5,384]{2,1,0:T(8,128)} %shard_map.136), calls=%async_computation | async-start | bytes 294912 | tf_op jit(solution)/shard_map/all_to_all | solution.py:248
  35.1 23.0 %copy-start.2 = (bf16[32,3072]{1,0:T(8,128)(2,1)S(1)}, bf16[32,3072]{1,0:T(8,128)(2,1)}, u32[]{:S(2)}) copy-start(bf16[32,3072]{1,0:T(8,128)(2,1)} %context.1) | copy-start | bytes 589828
  35.2 23.0 %copy-start.3 = (f32[3072]{0:T(1024)S(1)}, f32[3072]{0:T(1024)}, u32[]{:S(2)}) copy-start(f32[3072]{0:T(1024)} %param.21) | copy-start | bytes 36868
  35.2 33.5 %collective-permute-start.1 = (bf16[40,3072]{1,0:T(8,128)(2,1)S(1)}, bf16[40,3072]{1,0:T(8,128)(2,1)S(1)}, u32[]{:S(2)}, u32[]{:S(2)}) collective-permute-start(bf16[40,3072]{1,0:T(8,128)(2,1)S(1)} %collective-permute-done.refs_2_), channel_id=1, source_target_pairs={{0,8},{1,57},{2,10},{3,59},{4,12},{5,61},{6,14},{7,63},{8,16},{9,1... | collective-permute-start | bytes 737288 | tf_op jit(solution)/shard_map/ppermute | solution.py:271
  40.5 28.2 %collective-permute-start.6 = (bf16[40,3072]{1,0:T(8,128)(2,1)S(1)}, bf16[40,3072]{1,0:T(8,128)(2,1)S(1)}, u32[]{:S(2)}, u32[]{:S(2)}) collective-permute-start(bf16[40,3072]{1,0:T(8,128)(2,1)S(1)} %collective-permute-done.refs_2_), channel_id=1, source_target_pairs={{0,16},{1,49},{2,18},{3,51},{4,20},{5,53},{6,22},{7,55},{8,24},{9,... | collective-permute-start | bytes 737288 | tf_op jit(solution)/shard_map/ppermute | solution.py:271
  42.4 26.3 %collective-permute-start.5 = (bf16[40,3072]{1,0:T(8,128)(2,1)S(1)}, bf16[40,3072]{1,0:T(8,128)(2,1)S(1)}, u32[]{:S(2)}, u32[]{:S(2)}) collective-permute-start(bf16[40,3072]{1,0:T(8,128)(2,1)S(1)} %collective-permute-done.4.refs_6_), channel_id=1, source_target_pairs={{0,56},{1,9},{2,58},{3,11},{4,60},{5,13},{6,62},{7,15},{8,0},{9,17... | collective-permute-start | bytes 737288 | tf_op jit(solution)/shard_map/ppermute | solution.py:271
  46.4 11.7 %all-to-all-start.1 = ((f32[8,5,384]{2,1,0:T(8,128)}), f32[8,5,384]{2,1,0:T(8,128)S(1)}, u32[]{:S(2)}, u32[]{:S(2)}) async-start(f32[8,5,384]{2,1,0:T(8,128)} %shard_map.137), calls=%async_computation.1 | async-start | bytes 196608 | tf_op jit(solution)/shard_map/all_to_all | solution.py:248
  52.9 15.8 %copy-start = (bf16[40,3072]{1,0:T(8,128)(2,1)S(1)}, bf16[40,3072]{1,0:T(8,128)(2,1)}, u32[]{:S(2)}) copy-start(bf16[40,3072]{1,0:T(8,128)(2,1)} %refs_4_.1) | copy-start | bytes 737284
  59.2 21.9 %all-to-all-start.2 = ((bf16[12,32,128]{2,1,0:T(8,128)(2,1)}), bf16[12,32,128]{2,1,0:T(8,128)(2,1)S(1)}, u32[]{:S(2)}, u32[]{:S(2)}) async-start(bf16[12,32,128]{2,1,0:T(8,128)(2,1)} %shard_map.140), calls=%async_computation.2 | async-start | bytes 196608 | tf_op jit(solution)/shard_map/all_to_all | solution.py:248
  68.6 8.1 %copy-start.1 = (bf16[3072,384]{1,0:T(8,128)(2,1)S(1)}, bf16[3072,384]{1,0:T(8,128)(2,1)}, u32[]{:S(2)}) copy-start(bf16[3072,384]{1,0:T(8,128)(2,1)} %w_query.1) | copy-start | bytes 7077892
  71.4 8.3 %collective-permute-start.7 = (bf16[128,128]{1,0:T(8,128)(2,1)S(1)}, bf16[128,128]{1,0:T(8,128)(2,1)S(1)}, u32[]{:S(2)}, u32[]{:S(2)}) collective-permute-start(bf16[128,128]{1,0:T(8,128)(2,1)S(1)} %get-tuple-element.15), channel_id=1, source_target_pairs={{0,64},{64,128},{128,192},{192,256},{256,320},{320,384},{384,448},... | collective-permute-start | bytes 98312 | tf_op jit(solution)/shard_map/ppermute | solution.py:254
  75.3 5.8 %collective-permute-start.8 = (bf16[128,128]{1,0:T(8,128)(2,1)S(1)}, bf16[128,128]{1,0:T(8,128)(2,1)S(1)}, u32[]{:S(2)}, u32[]{:S(2)}) collective-permute-start(bf16[128,128]{1,0:T(8,128)(2,1)S(1)} %get-tuple-element.17), channel_id=1, source_target_pairs={{64,0},{128,64},{192,128},{256,192},{320,256},{384,320},{448,384},... | collective-permute-start | bytes 98312 | tf_op jit(solution)/shard_map/ppermute | solution.py:254
  76.7 4.3 %copy-start.4 = (f32[6]{0:T(128)S(1)}, f32[6]{0:T(128)}, u32[]{:S(2)}) copy-start(f32[6]{0:T(128)} %sink.1) | copy-start | bytes 76
  89.7 16.4 %collective-permute-start.11 = (bf16[40,3072]{1,0:T(8,128)(2,1)S(1)}, bf16[40,3072]{1,0:T(8,128)(2,1)S(1)}, u32[]{:S(2)}, u32[]{:S(2)}) collective-permute-start(bf16[40,3072]{1,0:T(8,128)(2,1)S(1)} %get-tuple-element.22), channel_id=1, source_target_pairs={{0,56},{1,9},{2,58},{3,11},{4,60},{5,13},{6,62},{7,15},{8,0},{9,17... | collective-permute-start | bytes 737288 | tf_op jit(solution)/shard_map/ppermute | solution.py:271
  93.2 13.0 %collective-permute-start.12 = (bf16[40,3072]{1,0:T(8,128)(2,1)S(1)}, bf16[40,3072]{1,0:T(8,128)(2,1)S(1)}, u32[]{:S(2)}, u32[]{:S(2)}) collective-permute-start(bf16[40,3072]{1,0:T(8,128)(2,1)S(1)} %get-tuple-element.21), channel_id=1, source_target_pairs={{0,8},{1,57},{2,10},{3,59},{4,12},{5,61},{6,14},{7,63},{8,16},{9,1... | collective-permute-start | bytes 737288 | tf_op jit(solution)/shard_map/ppermute | solution.py:271
  96.8 13.5 %collective-permute-start.13 = (bf16[40,3072]{1,0:T(8,128)(2,1)S(1)}, bf16[40,3072]{1,0:T(8,128)(2,1)S(1)}, u32[]{:S(2)}, u32[]{:S(2)}) collective-permute-start(bf16[40,3072]{1,0:T(8,128)(2,1)S(1)} %get-tuple-element.20), channel_id=1, source_target_pairs={{0,16},{1,49},{2,18},{3,51},{4,20},{5,53},{6,22},{7,55},{8,24},{9,... | collective-permute-start | bytes 737288 | tf_op jit(solution)/shard_map/ppermute | solution.py:271
  99.1 18.1 %collective-permute-start.10 = (bf16[40,3072]{1,0:T(8,128)(2,1)S(1)}, bf16[40,3072]{1,0:T(8,128)(2,1)S(1)}, u32[]{:S(2)}, u32[]{:S(2)}) collective-permute-start(bf16[40,3072]{1,0:T(8,128)(2,1)S(1)} %get-tuple-element.24), channel_id=1, source_target_pairs={{0,56},{1,9},{2,58},{3,11},{4,60},{5,13},{6,62},{7,15},{8,0},{9,17... | collective-permute-start | bytes 737288 | tf_op jit(solution)/shard_map/ppermute | solution.py:271
  102.1 15.0 %collective-permute-start.9 = (bf16[40,3072]{1,0:T(8,128)(2,1)S(1)}, bf16[40,3072]{1,0:T(8,128)(2,1)S(1)}, u32[]{:S(2)}, u32[]{:S(2)}) collective-permute-start(bf16[40,3072]{1,0:T(8,128)(2,1)S(1)} %get-tuple-element.19), channel_id=1, source_target_pairs={{0,8},{1,57},{2,10},{3,59},{4,12},{5,61},{6,14},{7,63},{8,16},{9,1... | collective-permute-start | bytes 737288 | tf_op jit(solution)/shard_map/ppermute | solution.py:271
  110.4 12.9 %collective-permute-start.14 = (bf16[40,3072]{1,0:T(8,128)(2,1)S(1)}, bf16[40,3072]{1,0:T(8,128)(2,1)S(1)}, u32[]{:S(2)}, u32[]{:S(2)}) collective-permute-start(bf16[40,3072]{1,0:T(8,128)(2,1)S(1)} %add_convert_fusion.1), channel_id=1, source_target_pairs={{0,16},{1,49},{2,18},{3,51},{4,20},{5,53},{6,22},{7,55},{8,24},{9,... | collective-permute-start | bytes 737288 | tf_op jit(solution)/shard_map/ppermute | solution.py:271
  114.3 12.3 %collective-permute-start.15 = (bf16[40,3072]{1,0:T(8,128)(2,1)S(1)}, bf16[40,3072]{1,0:T(8,128)(2,1)S(1)}, u32[]{:S(2)}, u32[]{:S(2)}) collective-permute-start(bf16[40,3072]{1,0:T(8,128)(2,1)S(1)} %add_convert_fusion.2), channel_id=1, source_target_pairs={{0,48},{1,17},{2,50},{3,19},{4,52},{5,21},{6,54},{7,23},{8,56},{9,... | collective-permute-start | bytes 737288 | tf_op jit(solution)/shard_map/ppermute | solution.py:271
  (2 other events, 4.9 us)
